TPU v7x, 128 devices: a whole 4x4x4 slice. The times are simulated.
128 devices in a mesh: sp: 32 (over z, y, core), tp: 4 (over x).
Axes of the slice: x: 4, y: 4, z: 4, core: 2. Of those that a mesh axis runs over, the one named last changes fastest.
Arguments:
- queries: bfloat16 [32768, 1024], P('sp', 'tp'), may hold values from -6 to 6
- keys: bfloat16 [32768, 1024], P('sp', 'tp'), may hold values from -6 to 6
- values: bfloat16 [32768, 1024], P('sp', 'tp'), may hold values from -6 to 6
- gates: bfloat16 [32768, 1024], P('sp', 'tp'), may hold values from -6 to 6
- log_decay: float32 [32768, 8], P('sp', 'tp'), may hold values from -1.6 to 0, as said below
- norm_gain: float32 [8, 128], P('tp'), may hold values from 0.1 to 1.9
- out_weight: bfloat16 [1024, 2048], P('tp'), may hold values from -0.1875 to 0.1875
- resid: bfloat16 [32768, 2048], P(('sp', 'tp')), may hold values from -6 to 6
- post_mix_gain: float32 [2048], replicated, may hold values from 0.1 to 1.9
- pre_ffn_gain: float32 [2048], replicated, may hold values from 0.1 to 1.9
- w_gate: bfloat16 [2048, 5632], P('sp', 'tp'), may hold values from -0.125 to 0.125
- w_up: bfloat16 [2048, 5632], P('sp', 'tp'), may hold values from -0.125 to 0.125
- w_down: bfloat16 [5632, 2048], P('tp', 'sp'), may hold values from -0.078125 to 0.078125
- post_ffn_gain: float32 [2048], replicated, may hold values from 0.1 to 1.9
Outputs:
- updated: bfloat16 [32768, 2048], P(('sp', 'tp'))
Inputs may be any that keep to these rules, and one draw needn't show every extreme that they name: `log_decay`: every entry is negative.
All inputs are finite; a program needn't handle non-finite values.
Results may differ from a plain program's by a relative error of at most 0.02.
Values may be sent and summed in bfloat16 or wider, within the bound.
A program may use at most 128 MiB of HBM per device.

v0:
```python
import jax
import jax.numpy as jnp
from jax import lax
from jax.sharding import Mesh
from jax.sharding import PartitionSpec as P

BLOCK = 512
SP = ("sp_0", "sp_1", "sp_2")
SP_TP = ("sp_0", "sp_1", "sp_2", "tp")


EPSILON = 1e-06


def filled_with(x, identity):
    return jax.tree.map(
        lambda part, zero: jnp.zeros_like(part) + jnp.asarray(zero, part.dtype), x, identity
    )


def entering(x, axes, combine, identity):
    before = start = filled_with(x, identity)
    subtotal = x
    for axis in reversed(axes):
        devices, index = (lax.axis_size(axis), lax.axis_index(axis))
        pieces = jax.tree.map(
            lambda part, kind: lax.all_gather(part.astype(kind), axis),
            subtotal,
            (jnp.bfloat16, jnp.bfloat16),
        )
        inside, subtotal = (start, start)
        for k in range(devices):
            passed = k < index
            subtotal = combine(
                subtotal, jax.tree.map(lambda part, own: part[k].astype(own.dtype), pieces, x)
            )
            inside = jax.tree.map(lambda new, old: jnp.where(passed, new, old), subtotal, inside)
        before = combine(inside, before)
    return before


def from_everyone(x, axis):
    devices = lax.axis_size(axis)
    return lax.all_to_all(jnp.broadcast_to(x[None], (devices, *x.shape)), axis, 0, 0, tiled=True)


def laid_out(blocks, dim):
    blocks = jnp.moveaxis(blocks, 0, dim)
    dims = blocks.shape
    return blocks.reshape(*dims[:dim], dims[dim] * dims[dim + 1], *dims[dim + 2 :])


def collect(x, axis, dim):
    blocks = from_everyone(x, axis)
    return laid_out(blocks, dim)


def side_by_side(arrays, axis, dim, along):
    both = jnp.concatenate(arrays, axis=along)
    out, at, outs = (lax.all_gather(both, axis, axis=dim, tiled=True), 0, [])
    for a in arrays:
        outs.append(lax.slice_in_dim(out, at, at + a.shape[along], axis=along))
        at += a.shape[along]
    return tuple(outs)


def rms_norm(values_in, gain_vec):
    widened = values_in.astype(jnp.float32)
    return (
        widened
        * lax.rsqrt(jnp.mean(widened * widened, axis=-1, keepdims=True) + EPSILON)
        * gain_vec
    )


def block_step(carried, pieces):
    query_blk, key_blk, value_blk, decay_blk = pieces
    length = query_blk.shape[1]
    key_scale = query_blk.shape[2] ** (-0.5)
    cumulative = jnp.cumsum(decay_blk, axis=1)
    log_gap = cumulative[:, :, None] - cumulative[:, None, :]
    causal = lax.broadcasted_iota(jnp.int32, (length, length), 0) >= lax.broadcasted_iota(
        jnp.int32, (length, length), 1
    )
    weight = jnp.where(causal[None], jnp.exp(jnp.minimum(log_gap, 0.0)), 0.0)
    products = jnp.einsum("htd,hsd->hts", query_blk, key_blk, preferred_element_type=jnp.float32)
    scores = (products * key_scale * weight).astype(jnp.bfloat16)
    within = jnp.einsum("hts,hsd->htd", scores, value_blk, preferred_element_type=jnp.float32)
    carried_term = (
        jnp.einsum(
            "htd,hde->hte", query_blk.astype(jnp.float32), carried, precision=lax.Precision.HIGHEST
        )
        * jnp.exp(cumulative)[:, :, None]
    )
    to_end = jnp.exp(cumulative[:, -1:] - cumulative) * key_scale
    scaled_keys = (key_blk.astype(jnp.float32) * to_end[:, :, None]).astype(jnp.bfloat16)
    added = jnp.einsum("hsd,hse->hde", scaled_keys, value_blk, preferred_element_type=jnp.float32)
    carried = jnp.exp(cumulative[:, -1])[:, None, None] * carried + added
    return (carried, within + carried_term)


def to_blocks(matrix, block_len, head_count):
    row_count = matrix.shape[0]
    return matrix.reshape(row_count // block_len, block_len, head_count, -1).transpose(0, 2, 1, 3)


def finish_heads(retention, gates, norm_gain):
    centered = retention - jnp.mean(retention, axis=-1, keepdims=True)
    variance = jnp.mean(centered * centered, axis=-1, keepdims=True)
    normed = centered * lax.rsqrt(variance + EPSILON) * norm_gain[None]
    gate_vals = gates.astype(jnp.float32).reshape(normed.shape)
    return (jax.nn.silu(gate_vals) * normed).reshape(normed.shape[0], -1).astype(jnp.bfloat16)


def combine_states(earlier, later):
    return (earlier[0] * later[0], later[0][:, None, None] * earlier[1] + later[1])


def per_device(
    queries,
    keys,
    values,
    gates,
    log_decay,
    norm_gain,
    out_weight,
    resid,
    post_mix_gain,
    pre_ffn_gain,
    w_gate,
    w_up,
    w_down,
    post_ffn_gain,
):
    row_count = queries.shape[0]
    head_count = log_decay.shape[1]
    head_dim = queries.shape[1] // head_count
    block_count = row_count // BLOCK
    query_blocks = to_blocks(queries, BLOCK, head_count)
    key_blocks = to_blocks(keys, BLOCK, head_count)
    value_blocks = to_blocks(values, BLOCK, head_count)
    decay_blocks = log_decay.reshape(block_count, BLOCK, head_count).transpose(0, 2, 1)
    start_state = jnp.zeros((head_count, head_dim, head_dim), jnp.float32)
    local_state, outputs = lax.scan(
        block_step, start_state, (query_blocks, key_blocks, value_blocks, decay_blocks)
    )
    retention = outputs.transpose(0, 2, 1, 3).reshape(row_count, head_count, head_dim)
    cumulative = jnp.cumsum(log_decay, axis=0)
    local_decay = jnp.exp(cumulative[-1])
    identity = (jnp.ones_like(local_decay), jnp.zeros_like(local_state))
    incoming = entering((local_decay, local_state), SP, combine_states, identity)
    query_rows = queries.reshape(row_count, head_count, head_dim).astype(jnp.float32)
    retention = (
        retention
        + jnp.einsum("thd,hde->the", query_rows, incoming[1], precision=lax.Precision.HIGHEST)
        * jnp.exp(cumulative)[:, :, None]
    )
    retained = finish_heads(retention, gates, norm_gain)
    quarter = resid.shape[0]
    regrouped = lax.all_to_all(retained, "tp", split_axis=0, concat_axis=1, tiled=True)
    group_rows = out_weight.shape[0]
    empty_mix = jnp.zeros((quarter, out_weight.shape[1]), jnp.float32)
    running = empty_mix
    shard_piece = collect(out_weight, "tp", 0)
    for offset in range(shard_piece.shape[0] // group_rows):
        columns = lax.dynamic_slice_in_dim(regrouped, offset * group_rows, group_rows, 1)
        part = jnp.dot(
            columns,
            shard_piece[offset * group_rows : (offset + 1) * group_rows],
            preferred_element_type=jnp.float32,
        )
        running = running + part.astype(jnp.bfloat16).astype(jnp.float32)
    mixed = running
    mixed = mixed.astype(jnp.bfloat16)
    middle = (resid.astype(jnp.float32) + rms_norm(mixed, post_mix_gain)).astype(jnp.bfloat16)
    ffn_input = rms_norm(middle, pre_ffn_gain).astype(jnp.bfloat16)
    gathered = collect(ffn_input, "tp", 0)
    shard_pieces = side_by_side((w_gate, w_up), SP, 0, 1)
    columns = gathered
    gate_act = jnp.dot(columns, shard_pieces[0], preferred_element_type=jnp.float32)
    up_act = jnp.dot(columns, shard_pieces[1], preferred_element_type=jnp.float32)
    down_full = lax.all_gather(w_down, SP, axis=1, tiled=True)
    hidden = (jax.nn.silu(gate_act) * up_act).astype(jnp.bfloat16)
    branch = lax.psum_scatter(
        jnp.dot(hidden, down_full, preferred_element_type=jnp.float32)
        .astype(jnp.bfloat16)
        .astype(jnp.float32)
        .astype(jnp.bfloat16),
        "tp",
        scatter_dimension=0,
        tiled=True,
    )
    return (middle.astype(jnp.float32) + rms_norm(branch, post_ffn_gain)).astype(jnp.bfloat16)


def solution(mesh):
    split = Mesh(mesh.devices.reshape(4, 4, 2, mesh.shape["tp"]), ("sp_0", "sp_1", "sp_2", "tp"))
    placed = (
        P(SP, "tp"),
        P(SP, "tp"),
        P(SP, "tp"),
        P(SP, "tp"),
        P(SP, "tp"),
        P("tp", None),
        P("tp", None),
        P(SP_TP, None),
        P(),
        P(),
        P(SP, "tp"),
        P(SP, "tp"),
        P("tp", SP),
        P(),
    )
    return jax.shard_map(
        per_device, mesh=split, in_specs=placed, out_specs=P(SP_TP, None), check_vma=False
    )
```

profile of v0, /device:TPU:1, one launch (start us, length us, event | category | flops | bytes accessed | tf_op | source)
XLA Modules:
  0.0 278.4 jit_solution(16982999338788517669)
XLA Ops:
  6.5 1.9 pad_maximum_fusion
  8.5 0.7 copy.95
  10.3 2.8 %all-gather.1 = bf16[2,1,2]{2,1,0:T(2,128)(2,1)S(1)} all-gather(bf16[1,1,2]{2,1,0:T(2,128)(2,1)S(1)} %bitcast.315), channel_id=1, replica_groups=mesh['sp_0'=4,'sp_1'=4,'sp_2'=2,'tp'=4] {'sp_2'}, dimensions={0}, use_global_device_ids=true | all-gather | bytes 12 | tf_op jit(solution)/shard_map/all_gather | solution.py:27
  13.2 8.1 %all-gather.2 = bf16[4,1,2]{2,1,0:T(2,128)(2,1)S(1)} all-gather(bf16[1,1,2]{2,1,0:T(2,128)(2,1)S(1)} %multiply_convert_fusion.5), channel_id=1, replica_groups=mesh['sp_0'=4,'sp_1'=4,'sp_2'=2,'tp'=4] {'sp_1'}, dimensions={0}, use_global_device_ids=true | all-gather | bytes 20 | tf_op jit(solution)/shard_map/all_gather | solution.py:27
  21.3 9.5 %all-gather.3 = bf16[4,1,2]{2,1,0:T(2,128)(2,1)S(1)} all-gather(bf16[1,1,2]{2,1,0:T(2,128)(2,1)S(1)} %fusion.134), channel_id=1, replica_groups=mesh['sp_0'=4,'sp_1'=4,'sp_2'=2,'tp'=4] {'sp_0'}, dimensions={0}, use_global_device_ids=true | all-gather | bytes 20 | tf_op jit(solution)/shard_map/all_gather | solution.py:27
  30.8 1.2 reshape.299
  32.3 1.2 copy.47
  33.4 9.5 %while.13 = (s32[]{:T(128)}, f32[2,128,128]{2,1,0:T(8,128)S(1)}, f32[2,2,512,128]{3,2,1,0:T(8,128)}, f32[2,2,512]{2,1,0:T(2,128)S(1)}, bf16[2,2,512,128]{3,1,2,0...) while((s32[]{:T(128)}, f32[2,128,128]{2,1,0:T(8,128)S(1)}, ...), condition=%wide.region_3.4_spmd.clone, body=%wide.region_0.3_spmd.clone.sunk | while | flops 507643936 | bytes 5702008 | solution.py:144
  35.4 1.0 fusion.154
  36.4 1.2 fusion.155
  38.2 0.6 reduce-window.26
  40.2 1.0 fusion.154
  41.2 1.2 fusion.155
  42.9 1.6 copy.51
  44.5 0.9 reshape.302
  45.4 5.4 %all-gather = bf16[4,128,128]{2,1,0:T(8,128)(2,1)S(1)} all-gather(bf16[2,128,128]{2,1,0:T(8,128)(2,1)S(1)} %convert_element_type.346), channel_id=2, replica_groups=mesh['sp_0'=4,'sp_1'=4,'sp_2'=2,'tp'=4] {'sp_2'}, dimensions={0}, use_global_device_ids=true | all-gather | bytes 196608 | tf_op jit(solution)/shard_map/all_gather | solution.py:27
  50.9 12.0 %all_gather.37 = bf16[4,2,128,128]{3,2,1,0:T(8,128)(2,1)S(1)} all-gather(bf16[1,2,128,128]{3,2,1,0:T(8,128)(2,1)S(1)} %fusion.79), channel_id=1, replica_groups=mesh['sp_0'=4,'sp_1'=4,'sp_2'=2,'tp'=4] {'sp_1'}, dimensions={0}, use_global_device_ids=true | all-gather | bytes 327680 | tf_op jit(solution)/shard_map/all_gather | solution.py:27
  63.1 11.0 %all_gather.38 = bf16[4,2,128,128]{3,2,1,0:T(8,128)(2,1)S(1)} all-gather(bf16[1,2,128,128]{3,2,1,0:T(8,128)(2,1)S(1)} %fusion.73), channel_id=1, replica_groups=mesh['sp_0'=4,'sp_1'=4,'sp_2'=2,'tp'=4] {'sp_0'}, dimensions={0}, use_global_device_ids=true | all-gather | bytes 327680 | tf_op jit(solution)/shard_map/all_gather | solution.py:27
  74.1 0.9 fusion.143
  76.1 0.9 copy.54
  76.9 4.0 %all-to-all-start = ((bf16[4,256,256]{1,2,0:T(8,128)(2,1)}), bf16[4,256,256]{1,2,0:T(8,128)(2,1)S(1)}, u32[]{:S(2)}, u32[]{:S(2)}) async-start(bf16[4,256,256]{1,2,0:T(8,128)(2,1)} %copy.54), calls=%async_computation | async-start | bytes 1048576 | tf_op jit(solution)/shard_map/all_to_all | solution.py:160
  81.0 0.7 all-gather.9.cloned.1.call-update
  81.7 6.2 %all-to-all-done = bf16[4,256,256]{1,2,0:T(8,128)(2,1)S(1)} async-done(((bf16[4,256,256]{1,2,0:T(8,128)(2,1)}), bf16[4,256,256]{1,2,0:T(8,128)(2,1)S(1)}, u32[]{:S(2)}, u32[]{:S(2)}) %all-to-all-start) | async-done | bytes 524320 | tf_op jit(solution)/shard_map/all_to_all | solution.py:160
  88.4 45.5 %all_to_all.26 = bf16[4,256,2048]{2,1,0:T(8,128)(2,1)S(1)} all-to-all(bf16[4,256,2048]{2,1,0:T(8,128)(2,1)S(1)} %broadcast_in_dim.27), channel_id=1, replica_groups=mesh['sp_0'=4,'sp_1'=4,'sp_2'=2,'tp'=4] {'tp'}, dimensions={0} | all-to-all | bytes 8388608 | tf_op jit(solution)/shard_map/all_to_all | solution.py:44
  135.3 0.8 fusion.38
  136.5 0.6 fusion.44
  138.0 45.5 %all_to_all.27 = bf16[4,256,2048]{2,1,0:T(8,128)(2,1)} all-to-all(bf16[4,256,2048]{2,1,0:T(8,128)(2,1)S(1)} %broadcast_in_dim.28), channel_id=1, replica_groups=mesh['sp_0'=4,'sp_1'=4,'sp_2'=2,'tp'=4] {'tp'}, dimensions={0} | all-to-all | bytes 8388608 | tf_op jit(solution)/shard_map/all_to_all | solution.py:44
  183.6 11.7 %fusion.19 = f32[1024,1408]{1,0:T(8,128)} fusion(bf16[1024,2048]{1,0:T(8,128)(2,1)} %bitcast.299, bf16[2048,2816]{1,0:T(8,128)(2,1)} %all-gather.7.cloned.1.call-done), kind=kOutput, calls=%fused_computation.36 | convolution fusion | flops 5905580032 | bytes 15728640 | tf_op jit(solution)/shard_map/dot_general | solution.py:180
  195.3 20.7 %fusion.26 = bf16[1024,2048]{1,0:T(8,128)(2,1)} fusion(bf16[1408,2048]{0,1:T(8,128)(2,1)} %all-gather.9.cloned.1.call-done, f32[1024,1408]{1,0:T(8,128)} %fusion.19, bf16[1024,2048]{1,0:T(8,128)(2,1)} %bitcast.300, bf16[2048,2816]{1,0:T(8,128)(2,1)} %all-gather.7.cloned.1.call-done), kind=kOutput, calls=%fused_computation.40 | convolution fusion | flops 11821907968 | bytes 25690112 | tf_op jit(solution)/shard_map/dot_general | solution.py:185
  216.0 51.8 %reduce-scatter.2.cloned.1.call-done = bf16[256,2048]{1,0:T(8,128)(2,1)} async-done(((bf16[1024,2048]{1,0:T(8,128)(2,1)}), bf16[256,2048]{1,0:T(8,128)(2,1)}) %reduce-scatter.2.cloned.1.call-update) | async-done | bytes 1048592 | tf_op jit(solution)/shard_map/reduce_scatter | solution.py:184
  267.7 1.5 fusion.42
  269.3 2.6 fusion.47
  (95 shorter events, 10.3 us)
Async XLA Ops:
  6.5 25.4 %copy-start.4 = (bf16[1024,256]{1,0:T(8,128)(2,1)S(1)}, bf16[1024,256]{1,0:T(8,128)(2,1)}, u32[]{:S(2)}) copy-start(bf16[1024,256]{1,0:T(8,128)(2,1)} %param.18) | copy-start | bytes 1572868
  6.5 25.6 %copy-start.5 = (bf16[1024,256]{1,0:T(8,128)(2,1)S(1)}, bf16[1024,256]{1,0:T(8,128)(2,1)}, u32[]{:S(2)}) copy-start(bf16[1024,256]{1,0:T(8,128)(2,1)} %param.16) | copy-start | bytes 1572868
  6.5 25.7 %copy-start.3 = (bf16[1024,256]{1,0:T(8,128)(2,1)S(1)}, bf16[1024,256]{1,0:T(8,128)(2,1)}, u32[]{:S(2)}) copy-start(bf16[1024,256]{1,0:T(8,128)(2,1)} %param.19) | copy-start | bytes 1572868
  6.5 177.0 %all-gather.7.cloned.1.call-start = ((), (), s32[]{:S(2)}) async-start(), calls=%async_computation.4 | async-start | bytes 11894784 | tf_op jit(solution)/shard_map/all_gather | solution.py:60
  32.0 1.5 copy-start.7
  44.5 29.6 %copy-start.6 = (bf16[1024,256]{1,0:T(8,128)(2,1)S(1)}, bf16[1024,256]{1,0:T(8,128)(2,1)}, u32[]{:S(2)}) copy-start(bf16[1024,256]{1,0:T(8,128)(2,1)} %param.16) | copy-start | bytes 1572868
  74.1 1.2 copy-start
  74.1 1.2 copy-start.11
  75.7 12.2 %copy-start.1 = (bf16[256,2048]{1,0:T(8,128)(2,1)S(1)}, bf16[256,2048]{1,0:T(8,128)(2,1)}, u32[]{:S(2)}) copy-start(bf16[256,2048]{1,0:T(8,128)(2,1)} %param.22) | copy-start | bytes 3145732
  76.9 10.9 %all-to-all-start = ((bf16[4,256,256]{1,2,0:T(8,128)(2,1)}), bf16[4,256,256]{1,2,0:T(8,128)(2,1)S(1)}, u32[]{:S(2)}, u32[]{:S(2)}) async-start(bf16[4,256,256]{1,2,0:T(8,128)(2,1)} %copy.54), calls=%async_computation | async-start | bytes 1048576 | tf_op jit(solution)/shard_map/all_to_all | solution.py:160
  81.0 114.3 %all-gather.9.cloned.1.call-start = ((), (), s32[]{:S(2)}) async-start(), calls=%async_computation.5 | async-start | bytes 5947392 | tf_op jit(solution)/shard_map/all_gather | solution.py:182
  81.7 186.0 %reduce-scatter.2.cloned.1.call-start = ((), (), s32[]{:S(2)}) async-start(), calls=%async_computation.6 | async-start | bytes 5242880 | tf_op jit(solution)/shard_map/reduce_scatter | solution.py:184
  135.3 1.2 copy-start.2
  135.3 1.2 copy-start.8
  136.1 1.1 copy-start.9
  216.0 53.3 %copy-start.10 = (f32[2048]{0:T(1024)S(1)}, f32[2048]{0:T(1024)}, u32[]{:S(2)}) copy-start(f32[2048]{0:T(1024)} %param.29) | copy-start | bytes 24580
Sparse Core Ops, SparseCore 0:
  9.6 65.6 all-gather.6
  84.0 51.0 all-gather.8
  216.1 51.5 reduce-scatter.1
where the time goes:
time: 279 us; the launch traced here: 278 us
  blocking collectives  140 us (50%)
  waiting for transfers between devices  58.7 us (21%)
  matrix products  40.9 us (15%)
  between operations  13.4 us (5%)
  other arithmetic  10.9 us (4%)
  local copies, waits for them, and re-layouts  10.6 us (4%)
  starting transfers between devices  4.05 us (1%)
    all_to_all x2, blocking collectives, from_everyone(): lax.all_to_all(jnp.broadcast_to(x[None], (devices, *x.shape)), axis, 0, 0...  91 us
    reduce_scatter x1, waiting for transfers between devices, per_device(): lax.psum_scatter(jnp.dot(hidden, down_full, preferred_element_type=jnp.fl...  51.8 us
    all_gather x6, blocking collectives, entering(): lax.all_gather(part.astype(kind), axis)  48.8 us
    dot_general x1, matrix products, per_device(): jnp.dot(hidden, down_full, preferred_element_type=jnp.float32)  20.7 us
    dot_general x1, matrix products, per_device(): jnp.dot(columns, shard_pieces[0], preferred_element_type=jnp.float32)  11.7 us
    all_to_all x1, waiting for transfers between devices, per_device(): lax.all_to_all(retained, 'tp', split_axis=0, concat_axis=1, tiled=True)  6.15 us
  transfers between devices with their start and end apart: 4, of which 2 were waited for; matrix products, arithmetic and copies ran while one was open for 13% of the time, Pallas kernels for 0%

commit v1 on v0

--- a/solution.py
+++ b/solution.py
@@ -1,6 +1,8 @@
 import jax
 import jax.numpy as jnp
 from jax import lax
+from jax.experimental import pallas as pl
+from jax.experimental.pallas import tpu as pltpu
 from jax.sharding import Mesh
 from jax.sharding import PartitionSpec as P
 
@@ -10,6 +12,281 @@
 
 
 EPSILON = 1e-06
+MESH_ID = pl.DeviceIdType.MESH
+Z, Y, C, X = SP_TP
+
+
+class Links:
+    def __init__(self, send_sem, recv_sem):
+        self.send_sem, self.recv_sem, self.copies = send_sem, recv_sem, []
+
+    def send(self, src, dst, **where):
+        at = len(self.copies)
+        copy = pltpu.make_async_remote_copy(
+            src_ref=src,
+            dst_ref=dst,
+            send_sem=self.send_sem.at[at],
+            recv_sem=self.recv_sem.at[at],
+            device_id={axis: index for axis, index in where.items()},
+            device_id_type=MESH_ID,
+        )
+        copy.start()
+        self.copies.append(copy)
+        return copy
+
+    def finish(self):
+        for copy in self.copies:
+            copy.wait_send()
+
+
+class PlaneGather:
+    def __init__(self, links, at, first, second, here, core):
+        self.links, self.at, self.first, self.second, self.core = links, at, first, second, core
+        self.i, self.j = here
+        self.i_up, self.i_down = lax.rem(self.i + 1, 4), lax.rem(self.i + 3, 4)
+        self.j_up, self.j_down = lax.rem(self.j + 1, 4), lax.rem(self.j + 3, 4)
+        self.across = []
+
+    def both_ways(self, axis, up, down, block):
+        return (
+            self.links.send(block, block, **{axis: up}),
+            self.links.send(block, block, **{axis: down}),
+        )
+
+    def own(self):
+        self.up, self.down = self.both_ways(
+            self.first, self.i_up, self.i_down, self.at(self.i, self.j)
+        )
+
+    def pass_on(self):
+        self.up.wait_recv()
+        block = self.at(self.i_down, self.j, part=0)
+        up = self.links.send(block, block, **{self.first: self.i_up})
+        self.down.wait_recv()
+        block = self.at(self.i_up, self.j, part=1)
+        self.up, self.down = up, self.links.send(block, block, **{self.first: self.i_down})
+
+    def give(self, j):
+        block = self.at(pl.ds(0, 4), j)
+        self.across.append(self.links.send(block, block, **{C: 1 - self.core}))
+
+    def line(self):
+        self.up.wait_recv()
+        self.down.wait_recv()
+        self.up, self.down = self.both_ways(
+            self.second, self.j_up, self.j_down, self.at(pl.ds(0, 4), self.j)
+        )
+        self.give(self.j)
+
+    def pass_line(self):
+        self.up.wait_recv()
+        block = self.at(pl.ds(0, 2), self.j_down)
+        up = self.links.send(block, block, **{self.second: self.j_up})
+        self.down.wait_recv()
+        block = self.at(pl.ds(2, 2), self.j_up)
+        down = self.links.send(block, block, **{self.second: self.j_down})
+        self.up, self.down = up, down
+        self.give(self.j_down)
+        self.give(self.j_up)
+
+    def end_line(self):
+        self.up.wait_recv()
+        self.down.wait_recv()
+        self.give(lax.rem(self.j + 2, 4))
+
+    def arrive(self):
+        for copy in self.across:
+            copy.wait_recv()
+
+
+def ffn_kernel(
+    ffn_in, middle, w_gate, w_up, w_down, gain, out,
+    gate_all, up_all, down_all, rows, hidden, partial, relay, final, half_down, local_sem, send_sem, recv_sem,
+):
+    z, y, c, x = (lax.axis_index(axis) for axis in SP_TP)
+    other, x_up, x_down, x_far = 1 - c, lax.rem(x + 1, 4), lax.rem(x + 3, 4), lax.rem(x + 2, 4)
+    copies = [
+        pltpu.make_async_copy(w_gate, gate_all.at[z, y, c], local_sem.at[0]),
+        pltpu.make_async_copy(w_up, up_all.at[z, y, c], local_sem.at[1]),
+        pltpu.make_async_copy(
+            w_down.at[pl.ds(pl.multiple_of(704 * c, 64), 704)], half_down.at[c], local_sem.at[2]
+        ),
+        pltpu.make_async_copy(ffn_in, rows.at[x], local_sem.at[3]),
+    ]
+    for copy in copies:
+        copy.start()
+
+    barrier = pltpu.get_barrier_semaphore()
+    near = [{C: other}]
+    for axis, index in ((X, x), (Y, y), (Z, z)):
+        near += [{axis: lax.rem(index + 1, 4)}, {axis: lax.rem(index + 3, 4)}]
+    for where in near:
+        pl.semaphore_signal(barrier, inc=1, device_id=where, device_id_type=MESH_ID)
+    pl.semaphore_wait(barrier, len(near))
+
+    links = Links(send_sem, recv_sem)
+    swap = links.send(
+        w_down.at[pl.ds(pl.multiple_of(704 * other, 64), 704)], half_down.at[c], **{C: other}
+    )
+
+    def gate_at(i, j, part=None):
+        lines = pl.ds(0, 64) if part is None else pl.ds(32 * part, 32)
+        return gate_all.at[j, i, c, lines]
+
+    def up_at(i, j, part=None):
+        lines = pl.ds(0, 64) if part is None else pl.ds(32 * part, 32)
+        return up_all.at[i, j, c, lines]
+
+    def down_lines(start, part):
+        first, length = (start, 352) if part is None else (start + 176 * part, 176)
+        return pl.ds(pl.multiple_of(704 * c + first, 16), length)
+
+    gathers = (
+        PlaneGather(links, gate_at, Y, Z, (y, z), c),
+        PlaneGather(links, up_at, Z, Y, (z, y), c),
+        PlaneGather(
+            links, lambda i, j, part=None: down_all.at[j, i, down_lines(0, part)], Y, Z, (y, z), c
+        ),
+        PlaneGather(
+            links, lambda i, j, part=None: down_all.at[i, j, down_lines(352, part)], Z, Y, (z, y), c
+        ),
+    )
+    wide, narrow = gathers[:2], gathers[2:]
+    copies[0].wait()
+    copies[1].wait()
+    for g in wide:
+        g.own()
+    copies[3].wait()
+    top, bottom = pl.ds(0, 128), pl.ds(128, 128)
+    up_top = links.send(rows.at[x, top], rows.at[x, top], **{X: x_up})
+    down_bottom = links.send(rows.at[x, bottom], rows.at[x, bottom], **{X: x_down})
+    copies[2].wait()
+    swap.wait_recv()
+    down_all[z, y, pl.ds(pl.multiple_of(704 * c, 64), 704), :] = jnp.concatenate(
+        [half_down[0], half_down[1]], axis=1
+    )
+    for g in wide:
+        g.pass_on()
+    for g in narrow:
+        g.own()
+    for g in wide:
+        g.line()
+    for g in narrow:
+        g.pass_on()
+    up_top.wait_recv()
+    far_top = links.send(rows.at[x_down, top], rows.at[x_down, top], **{X: x_up})
+    down_bottom.wait_recv()
+    far_bottom = links.send(rows.at[x_up, bottom], rows.at[x_up, bottom], **{X: x_down})
+    up_bottom = links.send(rows.at[x, bottom], rows.at[x, bottom], **{X: x_up})
+    down_top = links.send(rows.at[x, top], rows.at[x, top], **{X: x_down})
+    for g in narrow:
+        g.line()
+    for g in wide:
+        g.pass_line()
+    for g in wide:
+        g.end_line()
+    for g in narrow:
+        g.pass_line()
+    for g in wide:
+        g.arrive()
+
+    def gate_up(owner, slot):
+        block = rows[owner]
+        for j in range(11):
+            lanes = slice(128 * j, 128 * (j + 1))
+            weights = jnp.concatenate(
+                [
+                    gate_all[:, :, :, :, lanes].reshape(2048, 128),
+                    up_all[:, :, :, :, lanes].reshape(2048, 128),
+                ],
+                axis=1,
+            )
+            both = jnp.dot(block, weights, preferred_element_type=jnp.float32)
+            hidden[slot, :, lanes] = (jax.nn.silu(both[:, :128]) * both[:, 128:]).astype(jnp.bfloat16)
+
+    def down(slot, to, lines=pl.ds(0, 256), extra=None):
+        block = hidden[slot, lines, :]
+        for j in range(8):
+            weights = jnp.concatenate(
+                [down_all[j // 2, 2 * j % 4], down_all[j // 2, 2 * j % 4 + 1]], axis=1
+            )
+            part = jnp.dot(block, weights, preferred_element_type=jnp.float32)
+            lanes = slice(256 * j, 256 * (j + 1))
+            if extra is not None:
+                part = part + relay[extra, :, lanes].astype(jnp.float32)
+            partial[to, lines, lanes] = part.astype(jnp.bfloat16)
+
+    gate_up(x, 0)
+    far_top.wait_recv()
+    far_bottom.wait_recv()
+    gate_up(x_far, 1)
+    for g in narrow:
+        g.end_line()
+    for g in narrow:
+        g.arrive()
+    down(1, 1)
+    relay_up = links.send(partial.at[1, top], relay.at[0], **{X: x_up})
+    relay_down = links.send(partial.at[1, bottom], relay.at[1], **{X: x_down})
+    down(0, 0)
+    up_bottom.wait_recv()
+    down_top.wait_recv()
+    gate_up(x_up, 0)
+    down(0, 2, bottom)
+    last = [links.send(partial.at[2, bottom], final.at[0, bottom], **{X: x_up})]
+    gate_up(x_down, 1)
+    down(1, 3, top)
+    last.append(links.send(partial.at[3, top], final.at[1, top], **{X: x_down}))
+    relay_up.wait_recv()
+    down(0, 2, top, 0)
+    last.append(links.send(partial.at[2, top], final.at[0, top], **{X: x_up}))
+    relay_down.wait_recv()
+    down(1, 3, bottom, 1)
+    last.append(links.send(partial.at[3, bottom], final.at[1, bottom], **{X: x_down}))
+    for copy in last:
+        copy.wait_recv()
+
+    @pl.loop(0, 16)
+    def _(step):
+        lines = pl.ds(pl.multiple_of(16 * step, 16), 16)
+        branch = (
+            partial[0, lines, :].astype(jnp.float32)
+            + final[0, lines, :].astype(jnp.float32)
+            + final[1, lines, :].astype(jnp.float32)
+        ).astype(jnp.bfloat16)
+        out[lines, :] = (
+            middle[lines, :].astype(jnp.float32) + rms_norm(branch, gain[...])
+        ).astype(jnp.bfloat16)
+
+    links.finish()
+
+
+def feed_forward(ffn_in, middle, w_gate, w_up, w_down, gain):
+    in_hbm, in_vmem = pl.BlockSpec(memory_space=pl.ANY), pl.BlockSpec(memory_space=pltpu.VMEM)
+    bf16 = jnp.bfloat16
+    return pl.pallas_call(
+        ffn_kernel,
+        out_shape=jax.ShapeDtypeStruct((256, 2048), bf16),
+        in_specs=[in_hbm, in_vmem, in_hbm, in_hbm, in_hbm, in_vmem],
+        out_specs=in_vmem,
+        scratch_shapes=[
+            pltpu.VMEM((4, 4, 2, 64, 1408), bf16),
+            pltpu.VMEM((4, 4, 2, 64, 1408), bf16),
+            pltpu.VMEM((4, 4, 1408, 128), bf16),
+            pltpu.VMEM((4, 256, 2048), bf16),
+            pltpu.VMEM((2, 256, 1408), bf16),
+            pltpu.VMEM((4, 256, 2048), bf16),
+            pltpu.VMEM((2, 128, 2048), bf16),
+            pltpu.VMEM((2, 256, 2048), bf16),
+            pltpu.VMEM((2, 704, 64), bf16),
+            pltpu.SemaphoreType.DMA((4,)),
+            pltpu.SemaphoreType.DMA((72,)),
+            pltpu.SemaphoreType.DMA((72,)),
+        ],
+        compiler_params=pltpu.CompilerParams(
+            collective_id=0, has_side_effects=True, vmem_limit_bytes=60 * 2**20
+        ),
+        name="feed_forward",
+    )(ffn_in, middle, w_gate, w_up, w_down, gain)
 
 
 def filled_with(x, identity):
@@ -37,31 +314,6 @@
             inside = jax.tree.map(lambda new, old: jnp.where(passed, new, old), subtotal, inside)
         before = combine(inside, before)
     return before
-
-
-def from_everyone(x, axis):
-    devices = lax.axis_size(axis)
-    return lax.all_to_all(jnp.broadcast_to(x[None], (devices, *x.shape)), axis, 0, 0, tiled=True)
-
-
-def laid_out(blocks, dim):
-    blocks = jnp.moveaxis(blocks, 0, dim)
-    dims = blocks.shape
-    return blocks.reshape(*dims[:dim], dims[dim] * dims[dim + 1], *dims[dim + 2 :])
-
-
-def collect(x, axis, dim):
-    blocks = from_everyone(x, axis)
-    return laid_out(blocks, dim)
-
-
-def side_by_side(arrays, axis, dim, along):
-    both = jnp.concatenate(arrays, axis=along)
-    out, at, outs = (lax.all_gather(both, axis, axis=dim, tiled=True), 0, [])
-    for a in arrays:
-        outs.append(lax.slice_in_dim(out, at, at + a.shape[along], axis=along))
-        at += a.shape[along]
-    return tuple(outs)
 
 
 def rms_norm(values_in, gain_vec):
@@ -161,7 +413,7 @@
     group_rows = out_weight.shape[0]
     empty_mix = jnp.zeros((quarter, out_weight.shape[1]), jnp.float32)
     running = empty_mix
-    shard_piece = collect(out_weight, "tp", 0)
+    shard_piece = lax.all_gather(out_weight, "tp", axis=0, tiled=True)
     for offset in range(shard_piece.shape[0] // group_rows):
         columns = lax.dynamic_slice_in_dim(regrouped, offset * group_rows, group_rows, 1)
         part = jnp.dot(
@@ -174,23 +426,7 @@
     mixed = mixed.astype(jnp.bfloat16)
     middle = (resid.astype(jnp.float32) + rms_norm(mixed, post_mix_gain)).astype(jnp.bfloat16)
     ffn_input = rms_norm(middle, pre_ffn_gain).astype(jnp.bfloat16)
-    gathered = collect(ffn_input, "tp", 0)
-    shard_pieces = side_by_side((w_gate, w_up), SP, 0, 1)
-    columns = gathered
-    gate_act = jnp.dot(columns, shard_pieces[0], preferred_element_type=jnp.float32)
-    up_act = jnp.dot(columns, shard_pieces[1], preferred_element_type=jnp.float32)
-    down_full = lax.all_gather(w_down, SP, axis=1, tiled=True)
-    hidden = (jax.nn.silu(gate_act) * up_act).astype(jnp.bfloat16)
-    branch = lax.psum_scatter(
-        jnp.dot(hidden, down_full, preferred_element_type=jnp.float32)
-        .astype(jnp.bfloat16)
-        .astype(jnp.float32)
-        .astype(jnp.bfloat16),
-        "tp",
-        scatter_dimension=0,
-        tiled=True,
-    )
-    return (middle.astype(jnp.float32) + rms_norm(branch, post_ffn_gain)).astype(jnp.bfloat16)
+    return feed_forward(ffn_input, middle, w_gate, w_up, w_down, post_ffn_gain[None])
 
 
 def solution(mesh):

time: 279 us -> 202 us (0.72)
  Pallas kernels: 0 us -> 101 us
  blocking collectives: 140 us -> 45.7 us
  waiting for transfers between devices: 58.7 us -> 6.73 us
  matrix products: 40.9 us -> 11.1 us
  other arithmetic: 10.9 us -> 5.85 us
    pallas_call x0 -> x1, Pallas kernels: none -> 101 us  [feed_forward(): pl.pallas_call(ffn_kernel, out_shape=jax.ShapeDtypeStruct((256, 2048), bf...]
    all_to_all x2 -> x0, blocking collectives: 91 us -> none  [from_everyone(): lax.all_to_all(jnp.broadcast_to(x[None], (devices, *x.shape)), axis, 0, 0...]
    reduce_scatter x1 -> x0, waiting for transfers between devices: 51.8 us -> none  [per_device(): lax.psum_scatter(jnp.dot(hidden, down_full, preferred_element_type=jnp.fl...]
    dot_general x2 -> x0, matrix products: 32.4 us -> none  [the longest x1 20.7 us: per_device(): jnp.dot(hidden, down_full, preferred_element_type=jnp.float32)]
    unnamed x26 -> x28, local copies, waits for them, and re-layouts: 1.26 us -> 4.38 us
    all_gather x6, blocking collectives: 48.8 us -> 45.7 us  [entering(): lax.all_gather(part.astype(kind), axis)]
  transfers between devices with their start and end apart: 4 -> 2, of which waited for: 2 -> 1; matrix products, arithmetic and copies ran while one was open for 13% -> 10% of each run, Pallas kernels for 0% -> 0%
where the time goes in v1:
time: 202 us; the launch traced here: 200 us
  Pallas kernels  101 us (50%)
  blocking collectives  45.7 us (23%)
  between operations  13.7 us (7%)
  local copies, waits for them, and re-layouts  11.8 us (6%)
  matrix products  11.1 us (5%)
  waiting for transfers between devices  6.73 us (3%)
  other arithmetic  5.85 us (3%)
  starting transfers between devices  3.94 us (2%)
    pallas_call x1, Pallas kernels, feed_forward(): pl.pallas_call(ffn_kernel, out_shape=jax.ShapeDtypeStruct((256, 2048), bf...  101 us
    all_gather x6, blocking collectives, entering(): lax.all_gather(part.astype(kind), axis)  45.7 us
    all_to_all x1, waiting for transfers between devices, per_device(): lax.all_to_all(retained, 'tp', split_axis=0, concat_axis=1, tiled=True)  6.01 us
    dot_general x4, matrix products, per_device(): jnp.dot(columns, shard_piece[offset * group_rows:(offset + 1) * group_row...  4.75 us
    unnamed x28, local copies, waits for them, and re-layouts  4.38 us
  transfers between devices with their start and end apart: 2, of which 1 were waited for; matrix products, arithmetic and copies ran while one was open for 10% of the time, Pallas kernels for 0%

profile of v1, /device:TPU:1, one launch (start us, length us, event | category | flops | bytes accessed | tf_op | source)
XLA Modules:
  0.0 199.7 jit_solution(15104164311981208957)
XLA Ops:
  6.5 0.7 all-gather.6.cloned.1.call-update
  7.3 0.7 copy.99
  8.0 0.6 reduce-window.16
  9.2 2.8 %all-gather.1 = bf16[2,1,2]{2,1,0:T(2,128)(2,1)S(1)} all-gather(bf16[1,1,2]{2,1,0:T(2,128)(2,1)S(1)} %bitcast.297), channel_id=1, replica_groups=mesh['sp_0'=4,'sp_1'=4,'sp_2'=2,'tp'=4] {'sp_2'}, dimensions={0}, use_global_device_ids=true | all-gather | bytes 12 | tf_op jit(solution)/shard_map/all_gather | solution.py:304
  12.0 8.1 %all-gather.2 = bf16[4,1,2]{2,1,0:T(2,128)(2,1)S(1)} all-gather(bf16[1,1,2]{2,1,0:T(2,128)(2,1)S(1)} %multiply_convert_fusion.4), channel_id=1, replica_groups=mesh['sp_0'=4,'sp_1'=4,'sp_2'=2,'tp'=4] {'sp_1'}, dimensions={0}, use_global_device_ids=true | all-gather | bytes 20 | tf_op jit(solution)/shard_map/all_gather | solution.py:304
  20.1 1.2 reshape.280
  21.6 9.8 %all-gather.3 = bf16[4,1,2]{2,1,0:T(2,128)(2,1)S(1)} all-gather(bf16[1,1,2]{2,1,0:T(2,128)(2,1)S(1)} %fusion.122), channel_id=1, replica_groups=mesh['sp_0'=4,'sp_1'=4,'sp_2'=2,'tp'=4] {'sp_0'}, dimensions={0}, use_global_device_ids=true | all-gather | bytes 20 | tf_op jit(solution)/shard_map/all_gather | solution.py:304
  31.4 9.5 %while.13 = (s32[]{:T(128)}, f32[2,128,128]{2,1,0:T(8,128)S(1)}, f32[2,2,512,128]{3,2,1,0:T(8,128)}, f32[2,2,512]{2,1,0:T(2,128)S(1)}, bf16[2,2,512,128]{3,1,2,0...) while((s32[]{:T(128)}, f32[2,128,128]{2,1,0:T(8,128)S(1)}, ...), condition=%wide.region_3.4_spmd.clone, body=%wide.region_0.3_spmd.clone.sunk | while | flops 507643936 | bytes 5702508 | solution.py:396
  31.4 0.6 reduce-window.26
  33.1 1.0 fusion.138
  34.4 1.2 fusion.139
  35.6 0.5 convolution_add_fusion.2
  36.2 0.6 reduce-window.26
  37.9 1.0 fusion.138
  39.2 1.2 fusion.139
  40.9 1.6 copy.54
  42.6 0.9 reshape.283
  43.7 5.1 %all-gather = bf16[4,128,128]{2,1,0:T(8,128)(2,1)S(1)} all-gather(bf16[2,128,128]{2,1,0:T(8,128)(2,1)S(1)} %convert_element_type.331), channel_id=2, replica_groups=mesh['sp_0'=4,'sp_1'=4,'sp_2'=2,'tp'=4] {'sp_2'}, dimensions={0}, use_global_device_ids=true | all-gather | bytes 196608 | tf_op jit(solution)/shard_map/all_gather | solution.py:304
  48.9 10.6 %all_gather.34 = bf16[4,2,128,128]{3,2,1,0:T(8,128)(2,1)S(1)} all-gather(bf16[1,2,128,128]{3,2,1,0:T(8,128)(2,1)S(1)} %fusion.67), channel_id=1, replica_groups=mesh['sp_0'=4,'sp_1'=4,'sp_2'=2,'tp'=4] {'sp_1'}, dimensions={0}, use_global_device_ids=true | all-gather | bytes 327680 | tf_op jit(solution)/shard_map/all_gather | solution.py:304
  59.6 9.4 %all_gather.35 = bf16[4,2,128,128]{3,2,1,0:T(8,128)(2,1)S(1)} all-gather(bf16[1,2,128,128]{3,2,1,0:T(8,128)(2,1)S(1)} %fusion.61), channel_id=1, replica_groups=mesh['sp_0'=4,'sp_1'=4,'sp_2'=2,'tp'=4] {'sp_0'}, dimensions={0}, use_global_device_ids=true | all-gather | bytes 327680 | tf_op jit(solution)/shard_map/all_gather | solution.py:304
  69.0 0.9 fusion.130
  70.9 0.9 copy.57
  71.7 3.9 %all-to-all-start = ((bf16[4,256,256]{1,2,0:T(8,128)(2,1)}), bf16[4,256,256]{1,2,0:T(8,128)(2,1)S(1)}, u32[]{:S(2)}, u32[]{:S(2)}) async-start(bf16[4,256,256]{1,2,0:T(8,128)(2,1)} %copy.57), calls=%async_computation | async-start | bytes 1048576 | tf_op jit(solution)/shard_map/all_to_all | solution.py:412
  75.7 0.9 copy.58.w_down
  76.6 6.0 %all-to-all-done = bf16[4,256,256]{1,2,0:T(8,128)(2,1)S(1)} async-done(((bf16[4,256,256]{1,2,0:T(8,128)(2,1)}), bf16[4,256,256]{1,2,0:T(8,128)(2,1)S(1)}, u32[]{:S(2)}, u32[]{:S(2)}) %all-to-all-start) | async-done | bytes 524320 | tf_op jit(solution)/shard_map/all_to_all | solution.py:412
  82.6 1.8 fusion.22
  84.4 1.7 fusion.23
  86.6 0.8 fusion.25
  87.8 0.6 fusion.29
  88.5 1.3 fusion.31.ffn_in
  89.8 100.7 %feed_forward.1 = bf16[256,2048]{1,0:T(8,128)(2,1)} custom-call(bf16[256,2048]{1,0:T(8,128)(2,1)} %fusion.31.ffn_in, bf16[256,2048]{1,0:T(8,128)(2,1)} %copy-done, bf16[64,1408]{1,0:T(8,128)(2,1)} %w_gate.1, bf16[64,1408]{1,0:T(8,128)(2,1)} %w_up.1, bf16[1408,64]{1,0:T(8,128)(2,1)} %copy.58.w_down, f32[1,2048]{1,0:T(1,128)} %bitcast.294), custom_call_target="tpu_custom_call" | custom-call | tf_op jit(solution)/shard_map/feed_forward/pallas_call | solution.py:266
  190.5 2.3 %copy.129 = bf16[256,2048]{1,0:T(8,128)(2,1)} copy(bf16[256,2048]{1,0:T(8,128)(2,1)} %feed_forward.1) | data formatting | bytes 2097152
  (82 shorter events, 6.4 us)
Async XLA Ops:
  6.5 24.9 %copy-start.8 = (f32[1024,2]{0,1:T(2,128)S(1)}, f32[1024,2]{0,1:T(2,128)}, u32[]{:S(2)}) copy-start(f32[1024,2]{0,1:T(2,128)} %param.20) | copy-start | bytes 24580
  6.5 14.8 %copy-start.4 = (bf16[1024,256]{1,0:T(8,128)(2,1)S(1)}, bf16[1024,256]{1,0:T(8,128)(2,1)}, u32[]{:S(2)}) copy-start(bf16[1024,256]{1,0:T(8,128)(2,1)} %param.18) | copy-start | bytes 1572868
  6.5 14.9 %copy-start.5 = (bf16[1024,256]{1,0:T(8,128)(2,1)S(1)}, bf16[1024,256]{1,0:T(8,128)(2,1)}, u32[]{:S(2)}) copy-start(bf16[1024,256]{1,0:T(8,128)(2,1)} %param.16) | copy-start | bytes 1572868
  6.5 76.1 %all-gather.6.cloned.1.call-start = ((), (), s32[]{:S(2)}) async-start(), calls=%async_computation.1 | async-start | bytes 5242880 | tf_op jit(solution)/shard_map/all_gather | solution.py:416
  40.9 2.6 %copy-start.3 = (bf16[1024,256]{1,0:T(8,128)(2,1)S(1)}, bf16[1024,256]{1,0:T(8,128)(2,1)}, u32[]{:S(2)}) copy-start(bf16[1024,256]{1,0:T(8,128)(2,1)} %param.19) | copy-start | bytes 1572868
  42.5 26.4 %copy-start.6 = (bf16[1024,256]{1,0:T(8,128)(2,1)S(1)}, bf16[1024,256]{1,0:T(8,128)(2,1)}, u32[]{:S(2)}) copy-start(bf16[1024,256]{1,0:T(8,128)(2,1)} %param.16) | copy-start | bytes 1572868
  69.0 1.1 copy-start.11
  70.5 5.2 %copy-start.7 = (bf16[1408,64]{0,1:T(8,128)(2,1)S(1)}, bf16[1408,64]{0,1:T(8,128)(2,1)}, u32[]{:S(2)}) copy-start(bf16[1408,64]{0,1:T(8,128)(2,1)} %param.28) | copy-start | bytes 540676
  71.7 10.9 %all-to-all-start = ((bf16[4,256,256]{1,2,0:T(8,128)(2,1)}), bf16[4,256,256]{1,2,0:T(8,128)(2,1)S(1)}, u32[]{:S(2)}, u32[]{:S(2)}) async-start(bf16[4,256,256]{1,2,0:T(8,128)(2,1)} %copy.57), calls=%async_computation | async-start | bytes 1048576 | tf_op jit(solution)/shard_map/all_to_all | solution.py:412
  82.6 3.5 %copy-start.1 = (bf16[1024,2048]{1,0:T(8,128)(2,1)S(1)}, bf16[1024,2048]{1,0:T(8,128)(2,1)}, u32[]{:S(2)}) copy-start(bf16[1024,2048]{1,0:T(8,128)(2,1)} %all-gather.6.cloned.1.call-done) | copy-start | bytes 12582916
  86.6 1.2 copy-start.2
  86.6 1.2 copy-start.9
  87.4 1.1 copy-start.10
  88.5 1.3 copy-start
Sparse Core Ops, SparseCore 0:
  9.0 51.1 all-gather.5

commit v2 on v1

v2 whole, which is shorter than its diff:
```python
import jax
import jax.numpy as jnp
from jax import lax
from jax.experimental import pallas as pl
from jax.experimental.pallas import tpu as pltpu
from jax.sharding import Mesh
from jax.sharding import PartitionSpec as P

BLOCK = 512
SP = ("sp_0", "sp_1", "sp_2")
SP_TP = ("sp_0", "sp_1", "sp_2", "tp")


EPSILON = 1e-06
MESH_ID = pl.DeviceIdType.MESH
Z, Y, C, X = SP_TP


class Links:
    def __init__(self, send_sem, recv_sem):
        self.send_sem, self.recv_sem, self.copies = send_sem, recv_sem, []

    def send(self, src, dst, **where):
        at = len(self.copies)
        copy = pltpu.make_async_remote_copy(
            src_ref=src,
            dst_ref=dst,
            send_sem=self.send_sem.at[at],
            recv_sem=self.recv_sem.at[at],
            device_id={axis: index for axis, index in where.items()},
            device_id_type=MESH_ID,
        )
        copy.start()
        self.copies.append(copy)
        return copy

    def finish(self):
        for copy in self.copies:
            copy.wait_send()


class PlaneGather:
    def __init__(self, links, at, first, second, here, core):
        self.links, self.at, self.first, self.second, self.core = links, at, first, second, core
        self.i, self.j = here
        self.i_up, self.i_down = lax.rem(self.i + 1, 4), lax.rem(self.i + 3, 4)
        self.j_up, self.j_down = lax.rem(self.j + 1, 4), lax.rem(self.j + 3, 4)
        self.across = []

    def both_ways(self, axis, up, down, block):
        return (
            self.links.send(block, block, **{axis: up}),
            self.links.send(block, block, **{axis: down}),
        )

    def own(self):
        self.up, self.down = self.both_ways(
            self.first, self.i_up, self.i_down, self.at(self.i, self.j)
        )

    def pass_on(self):
        self.up.wait_recv()
        block = self.at(self.i_down, self.j, part=0)
        up = self.links.send(block, block, **{self.first: self.i_up})
        self.down.wait_recv()
        block = self.at(self.i_up, self.j, part=1)
        self.up, self.down = up, self.links.send(block, block, **{self.first: self.i_down})

    def give(self, j):
        block = self.at(pl.ds(0, 4), j)
        self.across.append(self.links.send(block, block, **{C: 1 - self.core}))

    def line(self):
        self.up.wait_recv()
        self.down.wait_recv()
        self.up, self.down = self.both_ways(
            self.second, self.j_up, self.j_down, self.at(pl.ds(0, 4), self.j)
        )
        self.give(self.j)

    def pass_line(self):
        self.up.wait_recv()
        block = self.at(pl.ds(0, 2), self.j_down)
        up = self.links.send(block, block, **{self.second: self.j_up})
        self.down.wait_recv()
        block = self.at(pl.ds(2, 2), self.j_up)
        down = self.links.send(block, block, **{self.second: self.j_down})
        self.up, self.down = up, down
        self.give(self.j_down)
        self.give(self.j_up)

    def end_line(self):
        self.up.wait_recv()
        self.down.wait_recv()
        self.give(lax.rem(self.j + 2, 4))

    def arrive(self):
        for copy in self.across:
            copy.wait_recv()


class LineGather(PlaneGather):
    def __init__(self, links, at, axis, index, core):
        super().__init__(links, lambda i, j, part=None: at(i, part), axis, axis, (index, index), core)

    def share(self, i):
        block = self.at(i, 0)
        self.across.append(self.links.send(block, block, **{C: 1 - self.core}))

    def pass_on(self):
        super().pass_on()
        for i in (self.i, self.i_down, self.i_up):
            self.share(i)

    def end(self):
        self.up.wait_recv()
        self.down.wait_recv()
        self.share(lax.rem(self.i + 2, 4))


def rms_norm(values_in, gain_vec):
    widened = values_in.astype(jnp.float32)
    return (
        widened
        * lax.rsqrt(jnp.mean(widened * widened, axis=-1, keepdims=True) + EPSILON)
        * gain_vec
    )


def over_lanes(scalar):
    return jnp.broadcast_to(scalar, (1, 128))


def write_state(ref, state, decay):
    ref[pl.ds(0, 128), :] = state[0].astype(jnp.bfloat16)
    ref[pl.ds(128, 128), :] = state[1].astype(jnp.bfloat16)
    row = lax.broadcasted_iota(jnp.int32, (16, 128), 0)
    large = [d.astype(jnp.bfloat16).astype(jnp.float32) for d in decay]
    both = jnp.where(
        row == 0,
        large[0],
        jnp.where(row == 1, decay[0] - large[0], jnp.where(row == 2, large[1], decay[1] - large[1])),
    )
    ref[pl.ds(256, 16), :] = both.astype(jnp.bfloat16)


def read_state(ref):
    both = ref[pl.ds(256, 16), :].astype(jnp.float32)
    return (
        [ref[pl.ds(128 * h, 128), :].astype(jnp.float32) for h in range(2)],
        [both[2 * h : 2 * h + 1] + both[2 * h + 1 : 2 * h + 2] for h in range(2)],
    )


def followed_by(earlier, later):
    return (
        [later[1][h] * earlier[0][h] + later[0][h] for h in range(2)],
        [later[1][h] * earlier[1][h] for h in range(2)],
    )


def chosen(which, a, b):
    return jax.tree.map(lambda p, q: jnp.where(which, p, q), a, b)


def layer_kernel(
    queries, keys, values, gates, log_decay, norm_gain, out_weight, resid, mix_gain, in_gain,
    w_gate, w_up, w_down, out_gain, out,
    gate_all, up_all, down_all, rows, hidden, partial, relay, final, half_down, turned,
    q, k, v, g, retention, decayed, state_c, state_y, state_z, retained, regrouped, out_all, middle,
    local_sem, send_sem, recv_sem,
):
    f32, bf16 = jnp.float32, jnp.bfloat16
    z, y, c, x = (lax.axis_index(axis) for axis in SP_TP)
    other, x_up, x_down, x_far = 1 - c, lax.rem(x + 1, 4), lax.rem(x + 3, 4), lax.rem(x + 2, 4)
    own_half = pl.ds(pl.multiple_of(704 * c, 64), 704)
    names = ("k", "v", "gate", "up", "q", "down", "weight", "g", "resid")
    moves = (
        (keys, k), (values, v), (w_gate, gate_all.at[z, y, c]), (w_up, up_all.at[z, y, c]), (queries, q),
        (w_down, half_down.at[c]), (out_weight, out_all.at[x]), (gates, g), (resid, middle),
    )
    local = {
        name: pltpu.make_async_copy(src, dst, local_sem.at[at])
        for at, (name, (src, dst)) in enumerate(zip(names, moves))
    }
    for copy in local.values():
        copy.start()

    barrier = pltpu.get_barrier_semaphore()
    near = [{C: other}]
    for axis, index in ((X, x), (Y, y), (Z, z)):
        near += [{axis: lax.rem(index + step, 4)} for step in (1, 2, 3)]
    for where in near:
        pl.semaphore_signal(barrier, inc=1, device_id=where, device_id_type=MESH_ID)
    pl.semaphore_wait(barrier, len(near))

    links = Links(send_sem, recv_sem)

    def gate_at(i, j, part=None):
        lines = pl.ds(0, 64) if part is None else pl.ds(32 * part, 32)
        return gate_all.at[j, i, c, lines]

    def up_at(i, j, part=None):
        lines = pl.ds(0, 64) if part is None else pl.ds(32 * part, 32)
        return up_all.at[i, j, c, lines]

    def down_lines(start, part):
        first, length = (start, 352) if part is None else (start + 176 * part, 176)
        return pl.ds(pl.multiple_of(704 * c + first, 16), length)

    def weight_at(i, part=None):
        first, length = (0, 128) if part is None else (64 * part, 64)
        return out_all.at[i, pl.ds(pl.multiple_of(128 * c + first, 64), length)]

    wide = (
        PlaneGather(links, gate_at, Y, Z, (y, z), c),
        PlaneGather(links, up_at, Z, Y, (z, y), c),
    )
    narrow = (
        PlaneGather(
            links, lambda i, j, part=None: down_all.at[j, i, down_lines(0, part)], Y, Z, (y, z), c
        ),
        PlaneGather(
            links, lambda i, j, part=None: down_all.at[i, j, down_lines(352, part)], Z, Y, (z, y), c
        ),
    )
    weight = LineGather(links, weight_at, X, x, c)

    scale = 128 ** (-0.5)
    at_row = lax.broadcasted_iota(jnp.int32, (BLOCK, BLOCK), 0)
    at_col = lax.broadcasted_iota(jnp.int32, (BLOCK, BLOCK), 1)
    upto = jnp.where(at_row <= at_col, 1.0, 0.0).astype(f32)
    cum_rows, cum_cols = [], []
    for b in range(2):
        logs = jnp.concatenate(
            [log_decay[:, BLOCK * b : BLOCK * (b + 1)], jnp.zeros((6, BLOCK), f32)], axis=0
        )
        cum = jnp.dot(logs, upto, precision=lax.Precision.HIGHEST, preferred_element_type=f32)
        cum_rows.append(cum)
        cum_cols.append(cum.T)
    ends = [[cum_rows[b][h : h + 1, BLOCK - 1 : BLOCK] for b in range(2)] for h in range(2)]
    local["k"].wait()
    local["v"].wait()
    first_state, span_state, span_decay = [], [], []
    for h in range(2):
        heads = slice(128 * h, 128 * (h + 1))
        added = []
        for b in range(2):
            lines = slice(BLOCK * b, BLOCK * (b + 1))
            to_end = jnp.exp(ends[h][b] - cum_cols[b][:, h : h + 1]) * scale
            scaled = (k[lines, heads].astype(f32) * to_end).astype(bf16)
            added.append(
                lax.dot_general(
                    scaled, v[lines, heads], (((0,), (0,)), ((), ())), preferred_element_type=f32
                )
            )
        first_state.append(added[0])
        span_state.append(jnp.exp(over_lanes(ends[h][1])) * added[0] + added[1])
        span_decay.append(jnp.exp(over_lanes(ends[h][0] + ends[h][1])))
    span = (span_state, span_decay)
    write_state(state_c.at[0], *span)
    pair = links.send(state_c.at[0], state_c.at[1], **{C: other})
    local["gate"].wait()
    local["up"].wait()
    for gather in wide:
        gather.own()
    local["weight"].wait()
    weight.own()
    local["down"].wait()
    swap = links.send(half_down.at[c], half_down.at[c], **{C: other})

    def within(h, b):
        heads, lines = slice(128 * h, 128 * (h + 1)), slice(BLOCK * b, BLOCK * (b + 1))
        col, row = cum_cols[b][:, h : h + 1], cum_rows[b][h : h + 1]
        products = lax.dot_general(
            q[lines, heads], k[lines, heads], (((1,), (1,)), ((), ())), preferred_element_type=f32
        )
        factor = jnp.where(at_row >= at_col, jnp.exp(jnp.minimum(col - row, 0.0)), 0.0)
        scores = (products * scale * factor).astype(bf16)
        result = jnp.dot(scores, v[lines, heads], preferred_element_type=f32)
        if b == 1:
            result = result + jnp.exp(col) * jnp.dot(
                q[lines, heads], first_state[h].astype(bf16), preferred_element_type=f32
            )
            col = col + ends[h][0]
        retention[h, lines, :] = result
        decayed[h, lines, :] = jnp.broadcast_to(jnp.exp(col), (BLOCK, 128))

    nothing = ([jnp.zeros((128, 128), f32)] * 2, [jnp.ones((1, 128), f32)] * 2)

    def among(slots, axis, index):
        sent = [
            links.send(slots.at[index], slots.at[index], **{axis: lax.rem(index + step, 4)})
            for step in (1, 2, 3)
        ]

        def fold():
            for copy in sent:
                copy.wait_recv()
            total, before = nothing, nothing
            for at in range(4):
                total = followed_by(total, read_state(slots.at[at]))
                before = chosen(at < index, total, before)
            return total, before

        return fold

    local["q"].wait()
    within(0, 0)
    pair.wait_recv()
    partner = read_state(state_c.at[1])
    first = c == 0
    chip = followed_by(chosen(first, span, partner), chosen(first, partner, span))
    before_core = chosen(first, nothing, partner)
    write_state(state_y.at[y], *chip)
    fold_y = among(state_y, Y, y)
    within(0, 1)
    for gather in wide:
        gather.pass_on()
    within(1, 0)
    line, before_y = fold_y()
    write_state(state_z.at[z], *line)
    fold_z = among(state_z, Z, z)
    swap.wait_recv()
    turned[...] = jnp.concatenate([half_down[0], half_down[1]], axis=0).T
    down_all[z, y, own_half, :] = turned[own_half, :]
    within(1, 1)
    for gather in narrow:
        gather.own()
    for gather in wide:
        gather.line()
    weight.pass_on()
    _, before_z = fold_z()
    entering = followed_by(followed_by(before_z, before_y), before_core)[0]
    entering = [state.astype(bf16) for state in entering]
    local["g"].wait()

    sent = []
    for step in (2, 1, 3, 0):
        quarter = lax.rem(x + step, 4)
        lines = pl.ds(pl.multiple_of(256 * quarter, 256), 256)
        for h in range(2):
            heads = slice(128 * h, 128 * (h + 1))
            carried = jnp.dot(q[lines, heads], entering[h], preferred_element_type=f32)
            value = retention[h, lines, :] + carried * decayed[h, lines, :]
            centered = value - jnp.mean(value, axis=-1, keepdims=True)
            variance = jnp.mean(centered * centered, axis=-1, keepdims=True)
            normed = centered * lax.rsqrt(variance + EPSILON) * norm_gain[h : h + 1, :]
            retained[quarter, :, heads] = (
                jax.nn.silu(g[lines, heads].astype(f32)) * normed
            ).astype(bf16)
        if step:
            sent.append(links.send(retained.at[quarter], regrouped.at[x], **{X: quarter}))
    for gather in narrow:
        gather.pass_on()
    weight.end()
    local["resid"].wait()
    for copy in weight.across:
        copy.wait_recv()
    for copy in sent:
        copy.wait_recv()

    for j in range(8):
        lanes = slice(256 * j, 256 * (j + 1))
        total = jnp.zeros((256, 256), f32)
        for step in range(4):
            owner = lax.rem(x + step, 4)
            block = regrouped[owner] if step else retained[x]
            part = jnp.dot(block, out_all[owner, :, lanes], preferred_element_type=f32)
            total = total + part.astype(bf16).astype(f32)
        partial[0, :, lanes] = total.astype(bf16)

    @pl.loop(0, 16)
    def _(step):
        lines = pl.ds(pl.multiple_of(16 * step, 16), 16)
        mid = (
            middle[lines, :].astype(f32) + rms_norm(partial[0, lines, :], mix_gain[...])
        ).astype(bf16)
        middle[lines, :] = mid
        rows[x, lines, :] = rms_norm(mid, in_gain[...]).astype(bf16)

    top, bottom = pl.ds(0, 128), pl.ds(128, 128)
    up_top = links.send(rows.at[x, top], rows.at[x, top], **{X: x_up})
    down_bottom = links.send(rows.at[x, bottom], rows.at[x, bottom], **{X: x_down})
    for gather in wide:
        gather.pass_line()
    for gather in narrow:
        gather.line()
    for gather in wide:
        gather.end_line()
    up_top.wait_recv()
    far_top = links.send(rows.at[x_down, top], rows.at[x_down, top], **{X: x_up})
    down_bottom.wait_recv()
    far_bottom = links.send(rows.at[x_up, bottom], rows.at[x_up, bottom], **{X: x_down})
    up_bottom = links.send(rows.at[x, bottom], rows.at[x, bottom], **{X: x_up})
    down_top = links.send(rows.at[x, top], rows.at[x, top], **{X: x_down})
    for gather in wide:
        gather.arrive()

    def gate_up(owner, slot):
        block = rows[owner]
        for j in range(11):
            lanes = slice(128 * j, 128 * (j + 1))
            weights = jnp.concatenate(
                [
                    gate_all[:, :, :, :, lanes].reshape(2048, 128),
                    up_all[:, :, :, :, lanes].reshape(2048, 128),
                ],
                axis=1,
            )
            both = jnp.dot(block, weights, preferred_element_type=f32)
            hidden[slot, :, lanes] = (jax.nn.silu(both[:, :128]) * both[:, 128:]).astype(bf16)

    def down(slot, to, lines=pl.ds(0, 256), extra=None):
        block = hidden[slot, lines, :]
        for j in range(8):
            weights = jnp.concatenate(
                [down_all[j // 2, 2 * j % 4], down_all[j // 2, 2 * j % 4 + 1]], axis=1
            )
            part = jnp.dot(block, weights, preferred_element_type=f32)
            lanes = slice(256 * j, 256 * (j + 1))
            if extra is not None:
                part = part + relay[extra, :, lanes].astype(f32)
            partial[to, lines, lanes] = part.astype(bf16)

    gate_up(x, 0)
    for gather in narrow:
        gather.pass_line()
    far_top.wait_recv()
    far_bottom.wait_recv()
    gate_up(x_far, 1)
    for gather in narrow:
        gather.end_line()
    for gather in narrow:
        gather.arrive()
    down(1, 1)
    relay_up = links.send(partial.at[1, top], relay.at[0], **{X: x_up})
    relay_down = links.send(partial.at[1, bottom], relay.at[1], **{X: x_down})
    down(0, 0)
    up_bottom.wait_recv()
    down_top.wait_recv()
    gate_up(x_up, 0)
    down(0, 2, bottom)
    last = [links.send(partial.at[2, bottom], final.at[0, bottom], **{X: x_up})]
    gate_up(x_down, 1)
    down(1, 3, top)
    last.append(links.send(partial.at[3, top], final.at[1, top], **{X: x_down}))
    relay_up.wait_recv()
    down(0, 2, top, 0)
    last.append(links.send(partial.at[2, top], final.at[0, top], **{X: x_up}))
    relay_down.wait_recv()
    down(1, 3, bottom, 1)
    last.append(links.send(partial.at[3, bottom], final.at[1, bottom], **{X: x_down}))
    for copy in last:
        copy.wait_recv()

    @pl.loop(0, 16)
    def _(step):
        lines = pl.ds(pl.multiple_of(16 * step, 16), 16)
        branch = (
            partial[0, lines, :].astype(f32)
            + final[0, lines, :].astype(f32)
            + final[1, lines, :].astype(f32)
        ).astype(bf16)
        out[lines, :] = (middle[lines, :].astype(f32) + rms_norm(branch, out_gain[...])).astype(bf16)

    links.finish()


def per_device(
    queries, keys, values, gates, log_decay, norm_gain, out_weight, resid, post_mix_gain, pre_ffn_gain,
    w_gate, w_up, w_down, post_ffn_gain,
):
    hbm, vmem = pl.BlockSpec(memory_space=pl.ANY), pl.BlockSpec(memory_space=pltpu.VMEM)
    f32, bf16 = jnp.float32, jnp.bfloat16
    return pl.pallas_call(
        layer_kernel,
        out_shape=jax.ShapeDtypeStruct((256, 2048), bf16),
        in_specs=[hbm, hbm, hbm, hbm, vmem, vmem, hbm, hbm, vmem, vmem, hbm, hbm, hbm, vmem],
        out_specs=vmem,
        scratch_shapes=[
            pltpu.VMEM((4, 4, 2, 64, 1408), bf16),
            pltpu.VMEM((4, 4, 2, 64, 1408), bf16),
            pltpu.VMEM((4, 4, 1408, 128), bf16),
            pltpu.VMEM((4, 256, 2048), bf16),
            pltpu.VMEM((2, 256, 1408), bf16),
            pltpu.VMEM((4, 256, 2048), bf16),
            pltpu.VMEM((2, 128, 2048), bf16),
            pltpu.VMEM((2, 256, 2048), bf16),
            pltpu.VMEM((2, 64, 1408), bf16),
            pltpu.VMEM((1408, 128), bf16),
            pltpu.VMEM((1024, 256), bf16),
            pltpu.VMEM((1024, 256), bf16),
            pltpu.VMEM((1024, 256), bf16),
            pltpu.VMEM((1024, 256), bf16),
            pltpu.VMEM((2, 1024, 128), f32),
            pltpu.VMEM((2, 1024, 128), f32),
            pltpu.VMEM((2, 272, 128), bf16),
            pltpu.VMEM((4, 272, 128), bf16),
            pltpu.VMEM((4, 272, 128), bf16),
            pltpu.VMEM((4, 256, 256), bf16),
            pltpu.VMEM((4, 256, 256), bf16),
            pltpu.VMEM((4, 256, 2048), bf16),
            pltpu.VMEM((256, 2048), bf16),
            pltpu.SemaphoreType.DMA((9,)),
            pltpu.SemaphoreType.DMA((96,)),
            pltpu.SemaphoreType.DMA((96,)),
        ],
        compiler_params=pltpu.CompilerParams(
            collective_id=0, has_side_effects=True, vmem_limit_bytes=60 * 2**20
        ),
        name="layer",
    )(
        queries, keys, values, gates, log_decay.T, norm_gain, out_weight, resid, post_mix_gain[None],
        pre_ffn_gain[None], w_gate, w_up, w_down.T, post_ffn_gain[None],
    )


def solution(mesh):
    split = Mesh(mesh.devices.reshape(4, 4, 2, mesh.shape["tp"]), ("sp_0", "sp_1", "sp_2", "tp"))
    placed = (
        P(SP, "tp"),
        P(SP, "tp"),
        P(SP, "tp"),
        P(SP, "tp"),
        P(SP, "tp"),
        P("tp", None),
        P("tp", None),
        P(SP_TP, None),
        P(),
        P(),
        P(SP, "tp"),
        P(SP, "tp"),
        P("tp", SP),
        P(),
    )
    return jax.shard_map(
        per_device, mesh=split, in_specs=placed, out_specs=P(SP_TP, None), check_vma=False
    )
```

time: 202 us -> 118 us (0.58); the launches traced: 200 us -> 118 us
  blocking collectives: 45.7 us -> 0 us
  Pallas kernels: 101 us -> 116 us
  between operations: 13.7 us -> 0.01 us
  matrix products: 11.1 us -> 0 us
  local copies, waits for them, and re-layouts: 11.8 us -> 2.3 us
  waiting for transfers between devices: 6.73 us -> 0 us
  other arithmetic: 5.85 us -> 0 us
  starting transfers between devices: 3.94 us -> 0 us
    all_gather x6 -> x0, blocking collectives: 45.7 us -> none  [entering(): lax.all_gather(part.astype(kind), axis)]
    pallas_call x1, Pallas kernels: 101 us -> 116 us  [per_device(): pl.pallas_call(layer_kernel, out_shape=jax.ShapeDtypeStruct((256, 2048),...]
    dot_general x11 -> x0, matrix products: 11.1 us -> none  [the longest x4 4.75 us: per_device(): jnp.dot(columns, shard_piece[offset * group_rows:(offset + 1) * group_row...]
    all_to_all x1 -> x0, waiting for transfers between devices: 6.01 us -> none  [per_device(): lax.all_to_all(retained, 'tp', split_axis=0, concat_axis=1, tiled=True)]
    all_to_all x1 -> x0, starting transfers between devices: 3.94 us -> none  [per_device(): lax.all_to_all(retained, 'tp', split_axis=0, concat_axis=1, tiled=True)]
    reshape x7 -> x0, local copies, waits for them, and re-layouts: 2.6 us -> none  [the longest x3 1.46 us: to_blocks(): matrix.reshape(row_count // block_len, block_len, head_count, -1)]
    another operation x6 -> x0, other arithmetic: 2.35 us -> none
    convert_element_type x10 -> x0, other arithmetic: 2.12 us -> none  [the longest x1 1.29 us: per_device(): ffn_input = rms_norm(middle, pre_ffn_gain).astype(jnp.bfloat16)]
  transfers between devices with their start and end apart: 2 -> 0, of which waited for: 1 -> 0; matrix products, arithmetic and copies ran while one was open for 10% -> 0% of each run, Pallas kernels for 0% -> 0%
where the time goes in v2:
time: 118 us
  Pallas kernels  116 us (98%)
  local copies, waits for them, and re-layouts  2.3 us (2%)
    pallas_call x1, Pallas kernels, per_device(): pl.pallas_call(layer_kernel, out_shape=jax.ShapeDtypeStruct((256, 2048),...  116 us

profile of v2, /device:TPU:1, one launch (start us, length us, event | category | flops | bytes accessed | tf_op | source)
XLA Modules:
  0.0 118.2 jit_solution(5277941376928516705)
XLA Ops:
  0.0 115.9 %layer.1 = bf16[256,2048]{1,0:T(8,128)(2,1)} custom-call(bf16[1024,256]{1,0:T(8,128)(2,1)} %queries.1, bf16[1024,256]{1,0:T(8,128)(2,1)} %keys.1, bf16[1024,256]{1,0:T(8,128)(2,1)} %values.1, bf16[1024,256]{1,0:T(8,128)(2,1)} %gates.1, f32[2,1024]{1,0:T(2,128)} %bitcast.6, f32[2,128]{1,0:T(2,128)} %norm_gain.1, bf16[256,2048]{1,0:T(8,128)(2,1)} %out_weight.1, ...), custom_call_target="tpu_custom_call" | custom-call | tf_op jit(solution)/shard_map/layer/pallas_call | solution.py:476
  115.9 2.3 %copy.16 = bf16[256,2048]{1,0:T(8,128)(2,1)} copy(bf16[256,2048]{1,0:T(8,128)(2,1)} %layer.1) | data formatting | bytes 2097152

commit v3 on v2

--- a/solution.py
+++ b/solution.py
@@ -76,46 +76,53 @@
         self.up, self.down = self.both_ways(
             self.second, self.j_up, self.j_down, self.at(pl.ds(0, 4), self.j)
         )
-        self.give(self.j)
 
     def pass_line(self):
         self.up.wait_recv()
-        block = self.at(pl.ds(0, 2), self.j_down)
-        up = self.links.send(block, block, **{self.second: self.j_up})
+        up = self.one_way(self.j_up, (0, 1), self.j_down)
         self.down.wait_recv()
-        block = self.at(pl.ds(2, 2), self.j_up)
-        down = self.links.send(block, block, **{self.second: self.j_down})
-        self.up, self.down = up, down
+        self.passed = (up, self.one_way(self.j_down, (2, 3), self.j_up))
         self.give(self.j_down)
         self.give(self.j_up)
 
+    def one_way(self, target, items, j):
+        blocks = [self.at(pl.ds(i, 1), j) for i in items]
+        return [self.links.send(block, block, **{self.second: target}) for block in blocks]
+
     def end_line(self):
-        self.up.wait_recv()
-        self.down.wait_recv()
-        self.give(lax.rem(self.j + 2, 4))
+        far = lax.rem(self.j + 2, 4)
+        for at in range(2):
+            for copies, start in zip(self.passed, (0, 2)):
+                copies[at].wait_recv()
+                block = self.at(pl.ds(start + at, 1), far)
+                self.across.append(self.links.send(block, block, **{C: 1 - self.core}))
 
     def arrive(self):
         for copy in self.across:
             copy.wait_recv()
 
 
-class LineGather(PlaneGather):
-    def __init__(self, links, at, axis, index, core):
-        super().__init__(links, lambda i, j, part=None: at(i, part), axis, axis, (index, index), core)
-
-    def share(self, i):
-        block = self.at(i, 0)
-        self.across.append(self.links.send(block, block, **{C: 1 - self.core}))
+class Ring:
+    def __init__(self, links, where, own, passed):
+        self.links, self.where, self.own, self.passed = links, where, own, passed
+
+    def both_ways(self, pairs, after=None):
+        copies = []
+        for at, (step, (src, dst)) in enumerate(zip((1, 3), pairs)):
+            if after:
+                after[at].wait_recv()
+            copies.append(self.links.send(src, dst, **self.where(step)))
+        return copies
+
+    def start(self):
+        self.copies = self.both_ways(self.own)
 
     def pass_on(self):
-        super().pass_on()
-        for i in (self.i, self.i_down, self.i_up):
-            self.share(i)
-
-    def end(self):
-        self.up.wait_recv()
-        self.down.wait_recv()
-        self.share(lax.rem(self.i + 2, 4))
+        self.copies = self.both_ways(self.passed, self.copies)
+
+    def finish(self):
+        for copy in self.copies:
+            copy.wait_recv()
 
 
 def rms_norm(values_in, gain_vec):
@@ -132,31 +139,19 @@
 
 
 def write_state(ref, state, decay):
-    ref[pl.ds(0, 128), :] = state[0].astype(jnp.bfloat16)
-    ref[pl.ds(128, 128), :] = state[1].astype(jnp.bfloat16)
+    ref[pl.ds(0, 128), :] = state.astype(jnp.bfloat16)
     row = lax.broadcasted_iota(jnp.int32, (16, 128), 0)
-    large = [d.astype(jnp.bfloat16).astype(jnp.float32) for d in decay]
-    both = jnp.where(
-        row == 0,
-        large[0],
-        jnp.where(row == 1, decay[0] - large[0], jnp.where(row == 2, large[1], decay[1] - large[1])),
-    )
-    ref[pl.ds(256, 16), :] = both.astype(jnp.bfloat16)
+    large = decay.astype(jnp.bfloat16).astype(jnp.float32)
+    ref[pl.ds(128, 16), :] = jnp.where(row == 0, large, decay - large).astype(jnp.bfloat16)
 
 
 def read_state(ref):
-    both = ref[pl.ds(256, 16), :].astype(jnp.float32)
-    return (
-        [ref[pl.ds(128 * h, 128), :].astype(jnp.float32) for h in range(2)],
-        [both[2 * h : 2 * h + 1] + both[2 * h + 1 : 2 * h + 2] for h in range(2)],
-    )
+    both = ref[pl.ds(128, 16), :].astype(jnp.float32)
+    return ref[pl.ds(0, 128), :].astype(jnp.float32), both[0:1] + both[1:2]
 
 
 def followed_by(earlier, later):
-    return (
-        [later[1][h] * earlier[0][h] + later[0][h] for h in range(2)],
-        [later[1][h] * earlier[1][h] for h in range(2)],
-    )
+    return later[1] * earlier[0] + later[0], later[1] * earlier[1]
 
 
 def chosen(which, a, b):
@@ -167,8 +162,8 @@
     queries, keys, values, gates, log_decay, norm_gain, out_weight, resid, mix_gain, in_gain,
     w_gate, w_up, w_down, out_gain, out,
     gate_all, up_all, down_all, rows, hidden, partial, relay, final, half_down, turned,
-    q, k, v, g, retention, decayed, state_c, state_y, state_z, retained, regrouped, out_all, middle,
-    local_sem, send_sem, recv_sem,
+    q, k, v, g, retention, decayed, state_c, state_y, state_z, state_in, retained, regrouped, passing, out_all, middle, result,
+    local_sem, out_sem, send_sem, recv_sem,
 ):
     f32, bf16 = jnp.float32, jnp.bfloat16
     z, y, c, x = (lax.axis_index(axis) for axis in SP_TP)
@@ -177,7 +172,7 @@
     names = ("k", "v", "gate", "up", "q", "down", "weight", "g", "resid")
     moves = (
         (keys, k), (values, v), (w_gate, gate_all.at[z, y, c]), (w_up, up_all.at[z, y, c]), (queries, q),
-        (w_down, half_down.at[c]), (out_weight, out_all.at[x]), (gates, g), (resid, middle),
+        (w_down, half_down.at[c]), (out_weight, out_all.at[0]), (gates, g), (resid, middle),
     )
     local = {
         name: pltpu.make_async_copy(src, dst, local_sem.at[at])
@@ -192,7 +187,6 @@
         near += [{axis: lax.rem(index + step, 4)} for step in (1, 2, 3)]
     for where in near:
         pl.semaphore_signal(barrier, inc=1, device_id=where, device_id_type=MESH_ID)
-    pl.semaphore_wait(barrier, len(near))
 
     links = Links(send_sem, recv_sem)
 
@@ -207,10 +201,6 @@
     def down_lines(start, part):
         first, length = (start, 352) if part is None else (start + 176 * part, 176)
         return pl.ds(pl.multiple_of(704 * c + first, 16), length)
-
-    def weight_at(i, part=None):
-        first, length = (0, 128) if part is None else (64 * part, 64)
-        return out_all.at[i, pl.ds(pl.multiple_of(128 * c + first, 64), length)]
 
     wide = (
         PlaneGather(links, gate_at, Y, Z, (y, z), c),
@@ -224,7 +214,39 @@
             links, lambda i, j, part=None: down_all.at[i, j, down_lines(352, part)], Z, Y, (z, y), c
         ),
     )
-    weight = LineGather(links, weight_at, X, x, c)
+
+    along = (1 - c) * y + c * z
+
+    def part_rows(i, part=None):
+        first, length = (0, 32) if part is None else (16 * part, 16)
+        return pl.ds(pl.multiple_of(128 * c + 32 * i + first, 16), length)
+
+    def on_line(step):
+        return {Y: lax.rem(y + (1 - c) * step, 4), Z: lax.rem(z + c * step, 4)}
+
+    weight_x = Ring(
+        links,
+        lambda step: {X: lax.rem(x + step, 4)},
+        (
+            (out_all.at[0, part_rows(along)], out_all.at[2, part_rows(along)]),
+            (out_all.at[0, part_rows(along)], out_all.at[1, part_rows(along)]),
+        ),
+        (
+            (out_all.at[2, part_rows(along, 0)], out_all.at[3, part_rows(along, 0)]),
+            (out_all.at[1, part_rows(along, 1)], out_all.at[3, part_rows(along, 1)]),
+        ),
+    )
+
+    def weight_ring(slots):
+        own, low, high = (
+            out_all.at[slots, part_rows(along)],
+            out_all.at[slots, part_rows(lax.rem(along + 3, 4), 0)],
+            out_all.at[slots, part_rows(lax.rem(along + 1, 4), 1)],
+        )
+        return Ring(links, on_line, ((own, own), (own, own)), ((low, low), (high, high)))
+
+    weight_near, weight_far = weight_ring(pl.ds(1, 2)), weight_ring(pl.ds(3, 1))
+    half_rows = pl.ds(pl.multiple_of(128 * c, 128), 128)
 
     scale = 128 ** (-0.5)
     at_row = lax.broadcasted_iota(jnp.int32, (BLOCK, BLOCK), 0)
@@ -241,7 +263,7 @@
     ends = [[cum_rows[b][h : h + 1, BLOCK - 1 : BLOCK] for b in range(2)] for h in range(2)]
     local["k"].wait()
     local["v"].wait()
-    first_state, span_state, span_decay = [], [], []
+    first_state, span = [], []
     for h in range(2):
         heads = slice(128 * h, 128 * (h + 1))
         added = []
@@ -255,19 +277,22 @@
                 )
             )
         first_state.append(added[0])
-        span_state.append(jnp.exp(over_lanes(ends[h][1])) * added[0] + added[1])
-        span_decay.append(jnp.exp(over_lanes(ends[h][0] + ends[h][1])))
-    span = (span_state, span_decay)
-    write_state(state_c.at[0], *span)
+        span.append(
+            (
+                jnp.exp(over_lanes(ends[h][1])) * added[0] + added[1],
+                jnp.exp(over_lanes(ends[h][0] + ends[h][1])),
+            )
+        )
+        write_state(state_c.at[0, h], *span[h])
+    pl.semaphore_wait(barrier, len(near))
     pair = links.send(state_c.at[0], state_c.at[1], **{C: other})
-    local["gate"].wait()
     local["up"].wait()
-    for gather in wide:
-        gather.own()
+    wide[1].own()
     local["weight"].wait()
-    weight.own()
+    weight_x.start()
     local["down"].wait()
     swap = links.send(half_down.at[c], half_down.at[c], **{C: other})
+    local["gate"].wait()
 
     def within(h, b):
         heads, lines = slice(128 * h, 128 * (h + 1)), slice(BLOCK * b, BLOCK * (b + 1))
@@ -286,12 +311,12 @@
         retention[h, lines, :] = result
         decayed[h, lines, :] = jnp.broadcast_to(jnp.exp(col), (BLOCK, 128))
 
-    nothing = ([jnp.zeros((128, 128), f32)] * 2, [jnp.ones((1, 128), f32)] * 2)
+    nothing = (jnp.zeros((128, 128), f32), jnp.ones((1, 128), f32))
 
     def among(slots, axis, index):
         sent = [
             links.send(slots.at[index], slots.at[index], **{axis: lax.rem(index + step, 4)})
-            for step in (1, 2, 3)
+            for step in (2, 1, 3)
         ]
 
         def fold():
@@ -308,15 +333,16 @@
     local["q"].wait()
     within(0, 0)
     pair.wait_recv()
-    partner = read_state(state_c.at[1])
+    partner = [read_state(state_c.at[1, h]) for h in range(2)]
     first = c == 0
-    chip = followed_by(chosen(first, span, partner), chosen(first, partner, span))
-    before_core = chosen(first, nothing, partner)
-    write_state(state_y.at[y], *chip)
+    chip = [
+        followed_by(chosen(first, span[h], partner[h]), chosen(first, partner[h], span[h]))
+        for h in range(2)
+    ]
+    write_state(state_y.at[y], *chosen(first, chip[0], chip[1]))
     fold_y = among(state_y, Y, y)
+    wide[0].own()
     within(0, 1)
-    for gather in wide:
-        gather.pass_on()
     within(1, 0)
     line, before_y = fold_y()
     write_state(state_z.at[z], *line)
@@ -325,16 +351,25 @@
     turned[...] = jnp.concatenate([half_down[0], half_down[1]], axis=0).T
     down_all[z, y, own_half, :] = turned[own_half, :]
     within(1, 1)
+    weight_x.pass_on()
+    weight_near.start()
+    _, before_z = fold_z()
+    state_in[c] = followed_by(before_z, before_y)[0]
+    both_heads = links.send(state_in.at[c], state_in.at[c], **{C: other})
+    weight_x.finish()
+    weight_far.start()
+    for gather in (wide[1], wide[0]):
+        gather.pass_on()
     for gather in narrow:
         gather.own()
-    for gather in wide:
-        gather.line()
-    weight.pass_on()
-    _, before_z = fold_z()
-    entering = followed_by(followed_by(before_z, before_y), before_core)[0]
-    entering = [state.astype(bf16) for state in entering]
     local["g"].wait()
-
+    both_heads.wait_recv()
+    entering = [
+        jnp.where(first, state_in[h], partner[h][1] * state_in[h] + partner[h][0]).astype(bf16)
+        for h in range(2)
+    ]
+
+    top, bottom = pl.ds(0, 128), pl.ds(128, 128)
     sent = []
     for step in (2, 1, 3, 0):
         quarter = lax.rem(x + step, 4)
@@ -346,54 +381,80 @@
             centered = value - jnp.mean(value, axis=-1, keepdims=True)
             variance = jnp.mean(centered * centered, axis=-1, keepdims=True)
             normed = centered * lax.rsqrt(variance + EPSILON) * norm_gain[h : h + 1, :]
-            retained[quarter, :, heads] = (
-                jax.nn.silu(g[lines, heads].astype(f32)) * normed
-            ).astype(bf16)
-        if step:
-            sent.append(links.send(retained.at[quarter], regrouped.at[x], **{X: quarter}))
+            retained[step, :, heads] = (jax.nn.silu(g[lines, heads].astype(f32)) * normed).astype(
+                bf16
+            )
+        if step == 2:
+            sent.append(links.send(retained.at[2, top], regrouped.at[3, top], **{X: x_far}))
+            to_pass = links.send(retained.at[2, bottom], passing, **{X: x_down})
+        elif step:
+            slot = 2 if step == 1 else 1
+            sent.append(links.send(retained.at[step], regrouped.at[slot], **{X: quarter}))
+    weight_near.pass_on()
+    weight_far.pass_on()
     for gather in narrow:
         gather.pass_on()
-    weight.end()
+    for gather in (wide[1], wide[0]):
+        gather.line()
+    to_pass.wait_recv()
+    sent.append(links.send(passing, regrouped.at[3, bottom], **{X: x_down}))
+    weight_near.finish()
+    near_half = out_all.at[pl.ds(1, 2), half_rows]
+    shared = [links.send(near_half, near_half, **{C: other})]
+    weight_far.finish()
+    far_half = out_all.at[3, half_rows]
+    shared.append(links.send(far_half, far_half, **{C: other}))
     local["resid"].wait()
-    for copy in weight.across:
+    for copy in sent:
         copy.wait_recv()
-    for copy in sent:
+    for copy in shared:
         copy.wait_recv()
 
     for j in range(8):
         lanes = slice(256 * j, 256 * (j + 1))
         total = jnp.zeros((256, 256), f32)
-        for step in range(4):
-            owner = lax.rem(x + step, 4)
-            block = regrouped[owner] if step else retained[x]
-            part = jnp.dot(block, out_all[owner, :, lanes], preferred_element_type=f32)
+        for slot in range(4):
+            block = regrouped[slot] if slot else retained[0]
+            part = jnp.dot(block, out_all[slot, :, lanes], preferred_element_type=f32)
             total = total + part.astype(bf16).astype(f32)
         partial[0, :, lanes] = total.astype(bf16)
 
-    @pl.loop(0, 16)
-    def _(step):
-        lines = pl.ds(pl.multiple_of(16 * step, 16), 16)
-        mid = (
-            middle[lines, :].astype(f32) + rms_norm(partial[0, lines, :], mix_gain[...])
-        ).astype(bf16)
-        middle[lines, :] = mid
-        rows[x, lines, :] = rms_norm(mid, in_gain[...]).astype(bf16)
-
-    top, bottom = pl.ds(0, 128), pl.ds(128, 128)
-    up_top = links.send(rows.at[x, top], rows.at[x, top], **{X: x_up})
-    down_bottom = links.send(rows.at[x, bottom], rows.at[x, bottom], **{X: x_down})
-    for gather in wide:
-        gather.pass_line()
+    piece = [pl.ds(64 * at, 64) for at in range(4)]
+    to_up, to_down = [], []
+    for at in range(2):
+
+        @pl.loop(0, 4)
+        def _(step):
+            for start in (64 * at, 64 * at + 128):
+                lines = pl.ds(pl.multiple_of(start + 16 * step, 16), 16)
+                mid = (
+                    middle[lines, :].astype(f32) + rms_norm(partial[0, lines, :], mix_gain[...])
+                ).astype(bf16)
+                middle[lines, :] = mid
+                rows[x, lines, :] = rms_norm(mid, in_gain[...]).astype(bf16)
+
+        for to, target, lines in ((to_up, x_up, piece[at]), (to_down, x_down, piece[2 + at])):
+            to.append(links.send(rows.at[x, lines], rows.at[x, lines], **{X: target}))
+    far, nearby = [], []
     for gather in narrow:
         gather.line()
+    for gather in (*wide, *narrow):
+        gather.give(gather.j)
+    forward = ((to_up, x_up, x_down, 0), (to_down, x_down, x_up, 2))
+    for at in range(2):
+        for to, target, source, start in forward:
+            to[at].wait_recv()
+            lines = piece[start + at]
+            far.append(links.send(rows.at[source, lines], rows.at[source, lines], **{X: target}))
+        if at == 0:
+            for gather in wide:
+                gather.pass_line()
+    for lines, target in ((bottom, x_up), (top, x_down)):
+        nearby.append(links.send(rows.at[x, lines], rows.at[x, lines], **{X: target}))
+    for gather in narrow:
+        gather.pass_line()
     for gather in wide:
         gather.end_line()
-    up_top.wait_recv()
-    far_top = links.send(rows.at[x_down, top], rows.at[x_down, top], **{X: x_up})
-    down_bottom.wait_recv()
-    far_bottom = links.send(rows.at[x_up, bottom], rows.at[x_up, bottom], **{X: x_down})
-    up_bottom = links.send(rows.at[x, bottom], rows.at[x, bottom], **{X: x_up})
-    down_top = links.send(rows.at[x, top], rows.at[x, top], **{X: x_down})
     for gather in wide:
         gather.arrive()
 
@@ -423,47 +484,59 @@
                 part = part + relay[extra, :, lanes].astype(f32)
             partial[to, lines, lanes] = part.astype(bf16)
 
-    gate_up(x, 0)
-    for gather in narrow:
-        gather.pass_line()
-    far_top.wait_recv()
-    far_bottom.wait_recv()
-    gate_up(x_far, 1)
+    for copy in far:
+        copy.wait_recv()
+    gate_up(x_far, 2)
     for gather in narrow:
         gather.end_line()
     for gather in narrow:
         gather.arrive()
-    down(1, 1)
+    down(2, 1)
     relay_up = links.send(partial.at[1, top], relay.at[0], **{X: x_up})
     relay_down = links.send(partial.at[1, bottom], relay.at[1], **{X: x_down})
-    down(0, 0)
-    up_bottom.wait_recv()
-    down_top.wait_recv()
+    for copy in nearby:
+        copy.wait_recv()
     gate_up(x_up, 0)
     down(0, 2, bottom)
     last = [links.send(partial.at[2, bottom], final.at[0, bottom], **{X: x_up})]
     gate_up(x_down, 1)
     down(1, 3, top)
     last.append(links.send(partial.at[3, top], final.at[1, top], **{X: x_down}))
+    gate_up(x, 2)
     relay_up.wait_recv()
     down(0, 2, top, 0)
-    last.append(links.send(partial.at[2, top], final.at[0, top], **{X: x_up}))
+    for at in range(2):
+        last.append(links.send(partial.at[2, piece[at]], final.at[0, piece[at]], **{X: x_up}))
     relay_down.wait_recv()
     down(1, 3, bottom, 1)
-    last.append(links.send(partial.at[3, bottom], final.at[1, bottom], **{X: x_down}))
-    for copy in last:
-        copy.wait_recv()
-
-    @pl.loop(0, 16)
-    def _(step):
-        lines = pl.ds(pl.multiple_of(16 * step, 16), 16)
-        branch = (
-            partial[0, lines, :].astype(f32)
-            + final[0, lines, :].astype(f32)
-            + final[1, lines, :].astype(f32)
-        ).astype(bf16)
-        out[lines, :] = (middle[lines, :].astype(f32) + rms_norm(branch, out_gain[...])).astype(bf16)
-
+    for at in range(2):
+        last.append(links.send(partial.at[3, piece[2 + at]], final.at[1, piece[2 + at]], **{X: x_down}))
+    down(2, 0)
+    written = []
+    last[0].wait_recv()
+    last[1].wait_recv()
+    for at in range(2):
+        last[2 + at].wait_recv()
+        last[4 + at].wait_recv()
+
+        @pl.loop(0, 4)
+        def _(step):
+            for start in (64 * at, 64 * at + 128):
+                lines = pl.ds(pl.multiple_of(start + 16 * step, 16), 16)
+                branch = (
+                    partial[0, lines, :].astype(f32)
+                    + final[0, lines, :].astype(f32)
+                    + final[1, lines, :].astype(f32)
+                ).astype(bf16)
+                result[lines, :] = (
+                    middle[lines, :].astype(f32) + rms_norm(branch, out_gain[...])
+                ).astype(bf16)
+
+        for lines in (piece[at], piece[2 + at]):
+            written.append(pltpu.make_async_copy(result.at[lines], out.at[lines], out_sem.at[len(written)]))
+            written[-1].start()
+    for copy in written:
+        copy.wait()
     links.finish()
 
 
@@ -477,13 +550,13 @@
         layer_kernel,
         out_shape=jax.ShapeDtypeStruct((256, 2048), bf16),
         in_specs=[hbm, hbm, hbm, hbm, vmem, vmem, hbm, hbm, vmem, vmem, hbm, hbm, hbm, vmem],
-        out_specs=vmem,
+        out_specs=hbm,
         scratch_shapes=[
             pltpu.VMEM((4, 4, 2, 64, 1408), bf16),
             pltpu.VMEM((4, 4, 2, 64, 1408), bf16),
             pltpu.VMEM((4, 4, 1408, 128), bf16),
             pltpu.VMEM((4, 256, 2048), bf16),
-            pltpu.VMEM((2, 256, 1408), bf16),
+            pltpu.VMEM((3, 256, 1408), bf16),
             pltpu.VMEM((4, 256, 2048), bf16),
             pltpu.VMEM((2, 128, 2048), bf16),
             pltpu.VMEM((2, 256, 2048), bf16),
@@ -495,16 +568,20 @@
             pltpu.VMEM((1024, 256), bf16),
             pltpu.VMEM((2, 1024, 128), f32),
             pltpu.VMEM((2, 1024, 128), f32),
-            pltpu.VMEM((2, 272, 128), bf16),
-            pltpu.VMEM((4, 272, 128), bf16),
-            pltpu.VMEM((4, 272, 128), bf16),
+            pltpu.VMEM((2, 2, 144, 128), bf16),
+            pltpu.VMEM((4, 144, 128), bf16),
+            pltpu.VMEM((4, 144, 128), bf16),
+            pltpu.VMEM((2, 128, 128), f32),
             pltpu.VMEM((4, 256, 256), bf16),
             pltpu.VMEM((4, 256, 256), bf16),
+            pltpu.VMEM((128, 256), bf16),
             pltpu.VMEM((4, 256, 2048), bf16),
             pltpu.VMEM((256, 2048), bf16),
+            pltpu.VMEM((256, 2048), bf16),
             pltpu.SemaphoreType.DMA((9,)),
-            pltpu.SemaphoreType.DMA((96,)),
-            pltpu.SemaphoreType.DMA((96,)),
+            pltpu.SemaphoreType.DMA((4,)),
+            pltpu.SemaphoreType.DMA((136,)),
+            pltpu.SemaphoreType.DMA((136,)),
         ],
         compiler_params=pltpu.CompilerParams(
             collective_id=0, has_side_effects=True, vmem_limit_bytes=60 * 2**20

time: 118 us -> 112 us (0.949); the launches traced: 118 us -> 111 us
  Pallas kernels: 116 us -> 108 us
    pallas_call x1, Pallas kernels: 116 us -> 108 us  [per_device(): pl.pallas_call(layer_kernel, out_shape=jax.ShapeDtypeStruct((256, 2048),...]
where the time goes in v3:
time: 112 us; the launch traced here: 111 us
  Pallas kernels  108 us (96%)
  local copies, waits for them, and re-layouts  2.3 us (2%)
    pallas_call x1, Pallas kernels, per_device(): pl.pallas_call(layer_kernel, out_shape=jax.ShapeDtypeStruct((256, 2048),...  108 us
    unnamed x1, local copies, waits for them, and re-layouts  2.3 us

profile of v3, /device:TPU:1, one launch (start us, length us, event | category | flops | bytes accessed | tf_op | source)
XLA Modules:
  0.0 110.7 jit_solution(6960816962743264582)
XLA Ops:
  0.0 108.4 %layer.1 = bf16[256,2048]{1,0:T(8,128)(2,1)} custom-call(bf16[1024,256]{1,0:T(8,128)(2,1)} %queries.1, bf16[1024,256]{1,0:T(8,128)(2,1)} %keys.1, bf16[1024,256]{1,0:T(8,128)(2,1)} %values.1, bf16[1024,256]{1,0:T(8,128)(2,1)} %gates.1, f32[2,1024]{1,0:T(2,128)} %bitcast.6, f32[2,128]{1,0:T(2,128)} %norm_gain.1, bf16[256,2048]{1,0:T(8,128)(2,1)} %out_weight.1, ...), custom_call_target="tpu_custom_call" | custom-call | tf_op jit(solution)/shard_map/layer/pallas_call | solution.py:549
  108.4 2.3 %copy.16 = bf16[256,2048]{1,0:T(8,128)(2,1)} copy(bf16[256,2048]{1,0:T(8,128)(2,1)} %layer.1) | data formatting | bytes 2097152

commit v4 on v3

--- a/solution.py
+++ b/solution.py
@@ -13,30 +13,52 @@
 
 EPSILON = 1e-06
 MESH_ID = pl.DeviceIdType.MESH
+SENDS, ARRIVALS = 40, 48
 Z, Y, C, X = SP_TP
+
+
+class Arrival:
+    def __init__(self, links, at):
+        self.links, self.at = links, at
+
+    def wait(self, as_large):
+        pltpu.make_async_remote_copy(
+            src_ref=as_large,
+            dst_ref=as_large,
+            send_sem=self.links.send_sem.at[0],
+            recv_sem=self.links.recv_sem.at[self.at],
+            device_id={X: lax.rem(lax.axis_index(X) + 1, 4)},
+            device_id_type=MESH_ID,
+        ).wait_recv()
 
 
 class Links:
     def __init__(self, send_sem, recv_sem):
-        self.send_sem, self.recv_sem, self.copies = send_sem, recv_sem, []
-
-    def send(self, src, dst, **where):
+        self.send_sem, self.recv_sem, self.copies, self.arrivals = send_sem, recv_sem, [], 0
+
+    def arrival(self):
+        self.arrivals += 1
+        return Arrival(self, self.arrivals - 1)
+
+    def send(self, arrival, src, dst, **where):
         at = len(self.copies)
+        if at >= SENDS:
+            self.copies[at - SENDS].wait_send()
         copy = pltpu.make_async_remote_copy(
             src_ref=src,
             dst_ref=dst,
-            send_sem=self.send_sem.at[at],
-            recv_sem=self.recv_sem.at[at],
+            send_sem=self.send_sem.at[at % SENDS],
+            recv_sem=self.recv_sem.at[arrival.at],
             device_id={axis: index for axis, index in where.items()},
             device_id_type=MESH_ID,
         )
         copy.start()
         self.copies.append(copy)
-        return copy
 
     def finish(self):
-        for copy in self.copies:
+        for copy in self.copies[-SENDS:]:
             copy.wait_send()
+        assert self.arrivals <= ARRIVALS
 
 
 class PlaneGather:
@@ -45,84 +67,81 @@
         self.i, self.j = here
         self.i_up, self.i_down = lax.rem(self.i + 1, 4), lax.rem(self.i + 3, 4)
         self.j_up, self.j_down = lax.rem(self.j + 1, 4), lax.rem(self.j + 3, 4)
-        self.across = []
-
-    def both_ways(self, axis, up, down, block):
-        return (
-            self.links.send(block, block, **{axis: up}),
-            self.links.send(block, block, **{axis: down}),
+        self.across = links.arrival()
+
+    def both_ways(self, axis, up, down, block_up, block_down):
+        arrival = self.links.arrival()
+        self.links.send(arrival, block_up, block_up, **{axis: up})
+        self.links.send(arrival, block_down, block_down, **{axis: down})
+        return arrival
+
+    def own(self):
+        block = self.at(self.i, self.j)
+        self.came = self.both_ways(self.first, self.i_up, self.i_down, block, block)
+
+    def pass_on(self):
+        self.came.wait(self.at(pl.ds(0, 2), self.j))
+        self.came = self.both_ways(
+            self.first,
+            self.i_up,
+            self.i_down,
+            self.at(self.i_down, self.j, part=0),
+            self.at(self.i_up, self.j, part=1),
         )
 
-    def own(self):
-        self.up, self.down = self.both_ways(
-            self.first, self.i_up, self.i_down, self.at(self.i, self.j)
-        )
-
-    def pass_on(self):
-        self.up.wait_recv()
-        block = self.at(self.i_down, self.j, part=0)
-        up = self.links.send(block, block, **{self.first: self.i_up})
-        self.down.wait_recv()
-        block = self.at(self.i_up, self.j, part=1)
-        self.up, self.down = up, self.links.send(block, block, **{self.first: self.i_down})
-
-    def give(self, j):
-        block = self.at(pl.ds(0, 4), j)
-        self.across.append(self.links.send(block, block, **{C: 1 - self.core}))
+    def give(self, j, items=pl.ds(0, 4)):
+        block = self.at(items, j)
+        self.links.send(self.across, block, block, **{C: 1 - self.core})
 
     def line(self):
-        self.up.wait_recv()
-        self.down.wait_recv()
-        self.up, self.down = self.both_ways(
-            self.second, self.j_up, self.j_down, self.at(pl.ds(0, 4), self.j)
-        )
+        self.came.wait(self.at(self.i, self.j))
+        block = self.at(pl.ds(0, 4), self.j)
+        self.came = self.both_ways(self.second, self.j_up, self.j_down, block, block)
 
     def pass_line(self):
-        self.up.wait_recv()
-        up = self.one_way(self.j_up, (0, 1), self.j_down)
-        self.down.wait_recv()
-        self.passed = (up, self.one_way(self.j_down, (2, 3), self.j_up))
+        self.came.wait(self.at(pl.ds(0, 4), pl.ds(0, 2)))
+        self.passed = [
+            self.both_ways(
+                self.second,
+                self.j_up,
+                self.j_down,
+                self.at(pl.ds(at, 1), self.j_down),
+                self.at(pl.ds(2 + at, 1), self.j_up),
+            )
+            for at in range(2)
+        ]
         self.give(self.j_down)
         self.give(self.j_up)
 
-    def one_way(self, target, items, j):
-        blocks = [self.at(pl.ds(i, 1), j) for i in items]
-        return [self.links.send(block, block, **{self.second: target}) for block in blocks]
-
     def end_line(self):
         far = lax.rem(self.j + 2, 4)
-        for at in range(2):
-            for copies, start in zip(self.passed, (0, 2)):
-                copies[at].wait_recv()
-                block = self.at(pl.ds(start + at, 1), far)
-                self.across.append(self.links.send(block, block, **{C: 1 - self.core}))
+        for at, arrival in enumerate(self.passed):
+            arrival.wait(self.at(pl.ds(0, 2), far))
+            for start in (0, 2):
+                self.give(far, pl.ds(start + at, 1))
 
     def arrive(self):
-        for copy in self.across:
-            copy.wait_recv()
+        self.across.wait(self.at(pl.ds(0, 4), pl.ds(0, 4)))
 
 
 class Ring:
-    def __init__(self, links, where, own, passed):
-        self.links, self.where, self.own, self.passed = links, where, own, passed
-
-    def both_ways(self, pairs, after=None):
-        copies = []
-        for at, (step, (src, dst)) in enumerate(zip((1, 3), pairs)):
-            if after:
-                after[at].wait_recv()
-            copies.append(self.links.send(src, dst, **self.where(step)))
-        return copies
+    def __init__(self, links, where, own, passed, as_large):
+        self.links, self.where, self.own, self.passed, self.as_large = links, where, own, passed, as_large
+
+    def both_ways(self, pairs):
+        self.came = self.links.arrival()
+        for step, (src, dst) in zip((1, 3), pairs):
+            self.links.send(self.came, src, dst, **self.where(step))
 
     def start(self):
-        self.copies = self.both_ways(self.own)
+        self.both_ways(self.own)
 
     def pass_on(self):
-        self.copies = self.both_ways(self.passed, self.copies)
+        self.came.wait(self.as_large[0])
+        self.both_ways(self.passed)
 
     def finish(self):
-        for copy in self.copies:
-            copy.wait_recv()
+        self.came.wait(self.as_large[1])
 
 
 def rms_norm(values_in, gain_vec):
@@ -162,17 +181,18 @@
     queries, keys, values, gates, log_decay, norm_gain, out_weight, resid, mix_gain, in_gain,
     w_gate, w_up, w_down, out_gain, out,
     gate_all, up_all, down_all, rows, hidden, partial, relay, final, half_down, turned,
-    q, k, v, g, retention, decayed, state_c, state_y, state_z, state_in, retained, regrouped, passing, out_all, middle, result,
-    local_sem, out_sem, send_sem, recv_sem,
+    q, k, v, g, retention, decayed, state_c, state_y, state_z, state_in, retained, regrouped, passing, out_all, middle, logs_in, gains, norm_in,
+    local_sem, send_sem, recv_sem,
 ):
     f32, bf16 = jnp.float32, jnp.bfloat16
     z, y, c, x = (lax.axis_index(axis) for axis in SP_TP)
     other, x_up, x_down, x_far = 1 - c, lax.rem(x + 1, 4), lax.rem(x + 3, 4), lax.rem(x + 2, 4)
     own_half = pl.ds(pl.multiple_of(704 * c, 64), 704)
-    names = ("k", "v", "gate", "up", "q", "down", "weight", "g", "resid")
+    names = ("logs", "k", "v", "gate", "up", "q", "down", "weight", "g", "resid", "mix", "in", "out", "norm")
     moves = (
-        (keys, k), (values, v), (w_gate, gate_all.at[z, y, c]), (w_up, up_all.at[z, y, c]), (queries, q),
+        (log_decay, logs_in), (keys, k), (values, v), (w_gate, gate_all.at[z, y, c]), (w_up, up_all.at[z, y, c]), (queries, q),
         (w_down, half_down.at[c]), (out_weight, out_all.at[0]), (gates, g), (resid, middle),
+        (mix_gain, gains.at[0]), (in_gain, gains.at[1]), (out_gain, gains.at[2]), (norm_gain, norm_in),
     )
     local = {
         name: pltpu.make_async_copy(src, dst, local_sem.at[at])
@@ -235,6 +255,7 @@
             (out_all.at[2, part_rows(along, 0)], out_all.at[3, part_rows(along, 0)]),
             (out_all.at[1, part_rows(along, 1)], out_all.at[3, part_rows(along, 1)]),
         ),
+        (out_all.at[pl.ds(1, 2), part_rows(along)], out_all.at[3, part_rows(along)]),
     )
 
     def weight_ring(slots):
@@ -243,7 +264,13 @@
             out_all.at[slots, part_rows(lax.rem(along + 3, 4), 0)],
             out_all.at[slots, part_rows(lax.rem(along + 1, 4), 1)],
         )
-        return Ring(links, on_line, ((own, own), (own, own)), ((low, low), (high, high)))
+        return Ring(
+            links,
+            on_line,
+            ((own, own), (own, own)),
+            ((low, low), (high, high)),
+            (out_all.at[slots, pl.ds(0, 64)], own),
+        )
 
     weight_near, weight_far = weight_ring(pl.ds(1, 2)), weight_ring(pl.ds(3, 1))
     half_rows = pl.ds(pl.multiple_of(128 * c, 128), 128)
@@ -253,9 +280,10 @@
     at_col = lax.broadcasted_iota(jnp.int32, (BLOCK, BLOCK), 1)
     upto = jnp.where(at_row <= at_col, 1.0, 0.0).astype(f32)
     cum_rows, cum_cols = [], []
+    local["logs"].wait()
     for b in range(2):
         logs = jnp.concatenate(
-            [log_decay[:, BLOCK * b : BLOCK * (b + 1)], jnp.zeros((6, BLOCK), f32)], axis=0
+            [logs_in[:, BLOCK * b : BLOCK * (b + 1)], jnp.zeros((6, BLOCK), f32)], axis=0
         )
         cum = jnp.dot(logs, upto, precision=lax.Precision.HIGHEST, preferred_element_type=f32)
         cum_rows.append(cum)
@@ -285,13 +313,15 @@
         )
         write_state(state_c.at[0, h], *span[h])
     pl.semaphore_wait(barrier, len(near))
-    pair = links.send(state_c.at[0], state_c.at[1], **{C: other})
+    pair = links.arrival()
+    links.send(pair, state_c.at[0], state_c.at[1], **{C: other})
     local["up"].wait()
     wide[1].own()
     local["weight"].wait()
     weight_x.start()
     local["down"].wait()
-    swap = links.send(half_down.at[c], half_down.at[c], **{C: other})
+    swap = links.arrival()
+    links.send(swap, half_down.at[c], half_down.at[c], **{C: other})
     local["gate"].wait()
 
     def within(h, b):
@@ -314,14 +344,12 @@
     nothing = (jnp.zeros((128, 128), f32), jnp.ones((1, 128), f32))
 
     def among(slots, axis, index):
-        sent = [
-            links.send(slots.at[index], slots.at[index], **{axis: lax.rem(index + step, 4)})
-            for step in (2, 1, 3)
-        ]
+        came = links.arrival()
+        for step in (2, 1, 3):
+            links.send(came, slots.at[index], slots.at[index], **{axis: lax.rem(index + step, 4)})
 
         def fold():
-            for copy in sent:
-                copy.wait_recv()
+            came.wait(slots.at[pl.ds(0, 3)])
             total, before = nothing, nothing
             for at in range(4):
                 total = followed_by(total, read_state(slots.at[at]))
@@ -332,7 +360,7 @@
 
     local["q"].wait()
     within(0, 0)
-    pair.wait_recv()
+    pair.wait(state_c.at[1])
     partner = [read_state(state_c.at[1, h]) for h in range(2)]
     first = c == 0
     chip = [
@@ -347,7 +375,7 @@
     line, before_y = fold_y()
     write_state(state_z.at[z], *line)
     fold_z = among(state_z, Z, z)
-    swap.wait_recv()
+    swap.wait(half_down.at[other])
     turned[...] = jnp.concatenate([half_down[0], half_down[1]], axis=0).T
     down_all[z, y, own_half, :] = turned[own_half, :]
     within(1, 1)
@@ -355,22 +383,24 @@
     weight_near.start()
     _, before_z = fold_z()
     state_in[c] = followed_by(before_z, before_y)[0]
-    both_heads = links.send(state_in.at[c], state_in.at[c], **{C: other})
+    both_heads = links.arrival()
+    links.send(both_heads, state_in.at[c], state_in.at[c], **{C: other})
     weight_x.finish()
     weight_far.start()
     for gather in (wide[1], wide[0]):
         gather.pass_on()
     for gather in narrow:
         gather.own()
-    local["g"].wait()
-    both_heads.wait_recv()
+    for name in ("g", "norm"):
+        local[name].wait()
+    both_heads.wait(state_in.at[other])
     entering = [
         jnp.where(first, state_in[h], partner[h][1] * state_in[h] + partner[h][0]).astype(bf16)
         for h in range(2)
     ]
 
     top, bottom = pl.ds(0, 128), pl.ds(128, 128)
-    sent = []
+    came, to_pass = links.arrival(), links.arrival()
     for step in (2, 1, 3, 0):
         quarter = lax.rem(x + step, 4)
         lines = pl.ds(pl.multiple_of(256 * quarter, 256), 256)
@@ -380,35 +410,35 @@
             value = retention[h, lines, :] + carried * decayed[h, lines, :]
             centered = value - jnp.mean(value, axis=-1, keepdims=True)
             variance = jnp.mean(centered * centered, axis=-1, keepdims=True)
-            normed = centered * lax.rsqrt(variance + EPSILON) * norm_gain[h : h + 1, :]
+            normed = centered * lax.rsqrt(variance + EPSILON) * norm_in[h : h + 1, :]
             retained[step, :, heads] = (jax.nn.silu(g[lines, heads].astype(f32)) * normed).astype(
                 bf16
             )
         if step == 2:
-            sent.append(links.send(retained.at[2, top], regrouped.at[3, top], **{X: x_far}))
-            to_pass = links.send(retained.at[2, bottom], passing, **{X: x_down})
+            links.send(came, retained.at[2, top], regrouped.at[3, top], **{X: x_far})
+            links.send(to_pass, retained.at[2, bottom], passing, **{X: x_down})
         elif step:
             slot = 2 if step == 1 else 1
-            sent.append(links.send(retained.at[step], regrouped.at[slot], **{X: quarter}))
+            links.send(came, retained.at[step], regrouped.at[slot], **{X: quarter})
     weight_near.pass_on()
     weight_far.pass_on()
     for gather in narrow:
         gather.pass_on()
     for gather in (wide[1], wide[0]):
         gather.line()
-    to_pass.wait_recv()
-    sent.append(links.send(passing, regrouped.at[3, bottom], **{X: x_down}))
+    to_pass.wait(passing)
+    links.send(came, passing, regrouped.at[3, bottom], **{X: x_down})
     weight_near.finish()
     near_half = out_all.at[pl.ds(1, 2), half_rows]
-    shared = [links.send(near_half, near_half, **{C: other})]
+    shared = links.arrival()
+    links.send(shared, near_half, near_half, **{C: other})
     weight_far.finish()
     far_half = out_all.at[3, half_rows]
-    shared.append(links.send(far_half, far_half, **{C: other}))
-    local["resid"].wait()
-    for copy in sent:
-        copy.wait_recv()
-    for copy in shared:
-        copy.wait_recv()
+    links.send(shared, far_half, far_half, **{C: other})
+    for name in ("resid", "mix", "in", "out"):
+        local[name].wait()
+    came.wait(regrouped.at[pl.ds(1, 3)])
+    shared.wait(out_all.at[pl.ds(1, 3), half_rows])
 
     for j in range(8):
         lanes = slice(256 * j, 256 * (j + 1))
@@ -420,7 +450,7 @@
         partial[0, :, lanes] = total.astype(bf16)
 
     piece = [pl.ds(64 * at, 64) for at in range(4)]
-    to_up, to_down = [], []
+    first_rows = [links.arrival(), links.arrival()]
     for at in range(2):
 
         @pl.loop(0, 4)
@@ -428,29 +458,27 @@
             for start in (64 * at, 64 * at + 128):
                 lines = pl.ds(pl.multiple_of(start + 16 * step, 16), 16)
                 mid = (
-                    middle[lines, :].astype(f32) + rms_norm(partial[0, lines, :], mix_gain[...])
+                    middle[lines, :].astype(f32) + rms_norm(partial[0, lines, :], gains[0])
                 ).astype(bf16)
                 middle[lines, :] = mid
-                rows[x, lines, :] = rms_norm(mid, in_gain[...]).astype(bf16)
-
-        for to, target, lines in ((to_up, x_up, piece[at]), (to_down, x_down, piece[2 + at])):
-            to.append(links.send(rows.at[x, lines], rows.at[x, lines], **{X: target}))
-    far, nearby = [], []
+                rows[x, lines, :] = rms_norm(mid, gains[1]).astype(bf16)
+
+        for target, lines in ((x_up, piece[at]), (x_down, piece[2 + at])):
+            links.send(first_rows[at], rows.at[x, lines], rows.at[x, lines], **{X: target})
     for gather in narrow:
         gather.line()
     for gather in (*wide, *narrow):
         gather.give(gather.j)
-    forward = ((to_up, x_up, x_down, 0), (to_down, x_down, x_up, 2))
+    far, nearby = links.arrival(), links.arrival()
     for at in range(2):
-        for to, target, source, start in forward:
-            to[at].wait_recv()
-            lines = piece[start + at]
-            far.append(links.send(rows.at[source, lines], rows.at[source, lines], **{X: target}))
+        first_rows[at].wait(rows.at[x, top])
+        for target, source, lines in ((x_up, x_down, piece[at]), (x_down, x_up, piece[2 + at])):
+            links.send(far, rows.at[source, lines], rows.at[source, lines], **{X: target})
         if at == 0:
             for gather in wide:
                 gather.pass_line()
     for lines, target in ((bottom, x_up), (top, x_down)):
-        nearby.append(links.send(rows.at[x, lines], rows.at[x, lines], **{X: target}))
+        links.send(nearby, rows.at[x, lines], rows.at[x, lines], **{X: target})
     for gather in narrow:
         gather.pass_line()
     for gather in wide:
@@ -484,40 +512,37 @@
                 part = part + relay[extra, :, lanes].astype(f32)
             partial[to, lines, lanes] = part.astype(bf16)
 
-    for copy in far:
-        copy.wait_recv()
+    far.wait(rows.at[x_far])
     gate_up(x_far, 2)
     for gather in narrow:
         gather.end_line()
     for gather in narrow:
         gather.arrive()
     down(2, 1)
-    relay_up = links.send(partial.at[1, top], relay.at[0], **{X: x_up})
-    relay_down = links.send(partial.at[1, bottom], relay.at[1], **{X: x_down})
-    for copy in nearby:
-        copy.wait_recv()
+    relay_up, relay_down = links.arrival(), links.arrival()
+    links.send(relay_up, partial.at[1, top], relay.at[0], **{X: x_up})
+    links.send(relay_down, partial.at[1, bottom], relay.at[1], **{X: x_down})
+    nearby.wait(rows.at[x_up])
     gate_up(x_up, 0)
     down(0, 2, bottom)
-    last = [links.send(partial.at[2, bottom], final.at[0, bottom], **{X: x_up})]
+    last = [links.arrival() for _ in range(3)]
+    links.send(last[2], partial.at[2, bottom], final.at[0, bottom], **{X: x_up})
     gate_up(x_down, 1)
     down(1, 3, top)
-    last.append(links.send(partial.at[3, top], final.at[1, top], **{X: x_down}))
+    links.send(last[2], partial.at[3, top], final.at[1, top], **{X: x_down})
     gate_up(x, 2)
-    relay_up.wait_recv()
+    relay_up.wait(relay.at[0])
     down(0, 2, top, 0)
     for at in range(2):
-        last.append(links.send(partial.at[2, piece[at]], final.at[0, piece[at]], **{X: x_up}))
-    relay_down.wait_recv()
+        links.send(last[at], partial.at[2, piece[at]], final.at[0, piece[at]], **{X: x_up})
+    relay_down.wait(relay.at[1])
     down(1, 3, bottom, 1)
     for at in range(2):
-        last.append(links.send(partial.at[3, piece[2 + at]], final.at[1, piece[2 + at]], **{X: x_down}))
+        links.send(last[at], partial.at[3, piece[2 + at]], final.at[1, piece[2 + at]], **{X: x_down})
     down(2, 0)
-    written = []
-    last[0].wait_recv()
-    last[1].wait_recv()
+    last[2].wait(final.at[0])
     for at in range(2):
-        last[2 + at].wait_recv()
-        last[4 + at].wait_recv()
+        last[at].wait(final.at[0, top])
 
         @pl.loop(0, 4)
         def _(step):
@@ -528,15 +553,10 @@
                     + final[0, lines, :].astype(f32)
                     + final[1, lines, :].astype(f32)
                 ).astype(bf16)
-                result[lines, :] = (
-                    middle[lines, :].astype(f32) + rms_norm(branch, out_gain[...])
+                out[lines, :] = (
+                    middle[lines, :].astype(f32) + rms_norm(branch, gains[2])
                 ).astype(bf16)
 
-        for lines in (piece[at], piece[2 + at]):
-            written.append(pltpu.make_async_copy(result.at[lines], out.at[lines], out_sem.at[len(written)]))
-            written[-1].start()
-    for copy in written:
-        copy.wait()
     links.finish()
 
 
@@ -544,13 +564,16 @@
     queries, keys, values, gates, log_decay, norm_gain, out_weight, resid, post_mix_gain, pre_ffn_gain,
     w_gate, w_up, w_down, post_ffn_gain,
 ):
-    hbm, vmem = pl.BlockSpec(memory_space=pl.ANY), pl.BlockSpec(memory_space=pltpu.VMEM)
     f32, bf16 = jnp.float32, jnp.bfloat16
+    operands = (
+        queries, keys, values, gates, log_decay.T, norm_gain, out_weight, resid, post_mix_gain[None],
+        pre_ffn_gain[None], w_gate, w_up, w_down.T, post_ffn_gain[None],
+    )
     return pl.pallas_call(
         layer_kernel,
         out_shape=jax.ShapeDtypeStruct((256, 2048), bf16),
-        in_specs=[hbm, hbm, hbm, hbm, vmem, vmem, hbm, hbm, vmem, vmem, hbm, hbm, hbm, vmem],
-        out_specs=hbm,
+        in_specs=[pl.BlockSpec(memory_space=pl.ANY)] * 14,
+        out_specs=pl.BlockSpec(memory_space=pltpu.VMEM),
         scratch_shapes=[
             pltpu.VMEM((4, 4, 2, 64, 1408), bf16),
             pltpu.VMEM((4, 4, 2, 64, 1408), bf16),
@@ -577,20 +600,18 @@
             pltpu.VMEM((128, 256), bf16),
             pltpu.VMEM((4, 256, 2048), bf16),
             pltpu.VMEM((256, 2048), bf16),
-            pltpu.VMEM((256, 2048), bf16),
-            pltpu.SemaphoreType.DMA((9,)),
-            pltpu.SemaphoreType.DMA((4,)),
-            pltpu.SemaphoreType.DMA((136,)),
-            pltpu.SemaphoreType.DMA((136,)),
+            pltpu.VMEM((2, 1024), f32),
+            pltpu.VMEM((3, 1, 2048), f32),
+            pltpu.VMEM((2, 128), f32),
+            pltpu.SemaphoreType.DMA((14,)),
+            pltpu.SemaphoreType.DMA((SENDS,)),
+            pltpu.SemaphoreType.DMA((ARRIVALS,)),
         ],
         compiler_params=pltpu.CompilerParams(
-            collective_id=0, has_side_effects=True, vmem_limit_bytes=60 * 2**20
+            collective_id=0, has_side_effects=True, vmem_limit_bytes=48 * 2**20
         ),
         name="layer",
-    )(
-        queries, keys, values, gates, log_decay.T, norm_gain, out_weight, resid, post_mix_gain[None],
-        pre_ffn_gain[None], w_gate, w_up, w_down.T, post_ffn_gain[None],
-    )
+    )(*(pltpu.with_memory_space_constraint(a, pltpu.HBM) for a in operands))
 
 
 def solution(mesh):

time: 112 us -> 107 us (0.955)
  Pallas kernels: 108 us -> 105 us
  local copies, waits for them, and re-layouts: 2.3 us -> 0.97 us
    pallas_call x1, Pallas kernels: 108 us -> 105 us  [per_device(): pl.pallas_call(layer_kernel, out_shape=jax.ShapeDtypeStruct((256, 2048),...]
    unnamed x1, local copies, waits for them, and re-layouts: 2.3 us -> 0.97 us
where the time goes in v4:
time: 107 us; the launch traced here: 106 us
  Pallas kernels  105 us (98%)
    pallas_call x1, Pallas kernels, per_device(): pl.pallas_call(layer_kernel, out_shape=jax.ShapeDtypeStruct((256, 2048),...  105 us

profile of v4, /device:TPU:1, one launch (start us, length us, event | category | flops | bytes accessed | tf_op | source)
XLA Modules:
  0.0 106.0 jit_solution(2483167152550286907)
XLA Ops:
  0.0 105.0 %layer.1 = bf16[256,2048]{1,0:T(8,128)(2,1)S(1)} custom-call(bf16[1024,256]{1,0:T(8,128)(2,1)} %queries.1, bf16[1024,256]{1,0:T(8,128)(2,1)} %keys.1, bf16[1024,256]{1,0:T(8,128)(2,1)} %values.1, bf16[1024,256]{1,0:T(8,128)(2,1)} %gates.1, f32[2,1024]{1,0:T(2,128)} %bitcast.6, f32[2,128]{1,0:T(2,128)} %norm_gain.1, bf16[256,2048]{1,0:T(8,128)(2,1)} %out_weight.1, ...), custom_call_target="tpu_custom_call" | custom-call | tf_op jit(solution)/shard_map/layer/pallas_call | solution.py:572
  105.0 1.0 copy.16

commit v5 on v4

--- a/solution.py
+++ b/solution.py
@@ -181,7 +181,7 @@
     queries, keys, values, gates, log_decay, norm_gain, out_weight, resid, mix_gain, in_gain,
     w_gate, w_up, w_down, out_gain, out,
     gate_all, up_all, down_all, rows, hidden, partial, relay, final, half_down, turned,
-    q, k, v, g, retention, decayed, state_c, state_y, state_z, state_in, retained, regrouped, passing, out_all, middle, logs_in, gains, norm_in,
+    q, k, v, g, retention, decayed, state_c, state_y, state_z, state_in, retained, regrouped, passing, out_all, mixed, middle, logs_in, gains, norm_in,
     local_sem, send_sem, recv_sem,
 ):
     f32, bf16 = jnp.float32, jnp.bfloat16
@@ -272,7 +272,15 @@
             (out_all.at[slots, pl.ds(0, 64)], own),
         )
 
-    weight_near, weight_far = weight_ring(pl.ds(1, 2)), weight_ring(pl.ds(3, 1))
+    weight_far = weight_ring(pl.ds(3, 1))
+    weight_rest = links.arrival()
+
+    def send_rest(steps):
+        for step in steps:
+            part = part_rows(lax.rem(along + step, 4))
+            for slot, target in ((2, x_up), (1, x_down)):
+                links.send(weight_rest, out_all.at[0, part], out_all.at[slot, part], **{X: target})
+
     half_rows = pl.ds(pl.multiple_of(128 * c, 128), 128)
 
     scale = 128 ** (-0.5)
@@ -319,6 +327,7 @@
     wide[1].own()
     local["weight"].wait()
     weight_x.start()
+    send_rest((1,))
     local["down"].wait()
     swap = links.arrival()
     links.send(swap, half_down.at[c], half_down.at[c], **{C: other})
@@ -380,15 +389,15 @@
     down_all[z, y, own_half, :] = turned[own_half, :]
     within(1, 1)
     weight_x.pass_on()
-    weight_near.start()
+    send_rest((2, 3))
+    wide[1].pass_on()
     _, before_z = fold_z()
     state_in[c] = followed_by(before_z, before_y)[0]
     both_heads = links.arrival()
     links.send(both_heads, state_in.at[c], state_in.at[c], **{C: other})
+    wide[0].pass_on()
     weight_x.finish()
     weight_far.start()
-    for gather in (wide[1], wide[0]):
-        gather.pass_on()
     for gather in narrow:
         gather.own()
     for name in ("g", "norm"):
@@ -400,7 +409,7 @@
     ]
 
     top, bottom = pl.ds(0, 128), pl.ds(128, 128)
-    came, to_pass = links.arrival(), links.arrival()
+    near_came, far_came, to_pass = (links.arrival() for _ in range(3))
     for step in (2, 1, 3, 0):
         quarter = lax.rem(x + step, 4)
         lines = pl.ds(pl.multiple_of(256 * quarter, 256), 256)
@@ -415,47 +424,50 @@
                 bf16
             )
         if step == 2:
-            links.send(came, retained.at[2, top], regrouped.at[3, top], **{X: x_far})
+            links.send(far_came, retained.at[2, top], regrouped.at[3, top], **{X: x_far})
             links.send(to_pass, retained.at[2, bottom], passing, **{X: x_down})
         elif step:
             slot = 2 if step == 1 else 1
-            links.send(came, retained.at[step], regrouped.at[slot], **{X: quarter})
-    weight_near.pass_on()
+            links.send(near_came, retained.at[step], regrouped.at[slot], **{X: quarter})
     weight_far.pass_on()
     for gather in narrow:
         gather.pass_on()
     for gather in (wide[1], wide[0]):
         gather.line()
     to_pass.wait(passing)
-    links.send(came, passing, regrouped.at[3, bottom], **{X: x_down})
-    weight_near.finish()
-    near_half = out_all.at[pl.ds(1, 2), half_rows]
-    shared = links.arrival()
+    links.send(far_came, passing, regrouped.at[3, bottom], **{X: x_down})
+    shared, shared_far = links.arrival(), links.arrival()
+    weight_rest.wait(out_all.at[pl.ds(1, 2), pl.ds(0, 96)])
+    near_half, far_half = out_all.at[pl.ds(1, 2), half_rows], out_all.at[3, half_rows]
     links.send(shared, near_half, near_half, **{C: other})
     weight_far.finish()
-    far_half = out_all.at[3, half_rows]
-    links.send(shared, far_half, far_half, **{C: other})
+    links.send(shared_far, far_half, far_half, **{C: other})
     for name in ("resid", "mix", "in", "out"):
         local[name].wait()
-    came.wait(regrouped.at[pl.ds(1, 3)])
-    shared.wait(out_all.at[pl.ds(1, 3), half_rows])
+    near_came.wait(regrouped.at[pl.ds(1, 2)])
+    shared.wait(out_all.at[pl.ds(1, 2), half_rows])
+
+    def mix_part(slot, lanes):
+        block = regrouped[slot] if slot else retained[0]
+        part = jnp.dot(block, out_all[slot, :, lanes], preferred_element_type=f32)
+        return part.astype(bf16).astype(f32)
 
     for j in range(8):
         lanes = slice(256 * j, 256 * (j + 1))
-        total = jnp.zeros((256, 256), f32)
-        for slot in range(4):
-            block = regrouped[slot] if slot else retained[0]
-            part = jnp.dot(block, out_all[slot, :, lanes], preferred_element_type=f32)
-            total = total + part.astype(bf16).astype(f32)
-        partial[0, :, lanes] = total.astype(bf16)
+        mixed[:, lanes] = mix_part(0, lanes) + mix_part(1, lanes) + mix_part(2, lanes)
+    far_came.wait(regrouped.at[3])
+    shared_far.wait(out_all.at[3, half_rows])
+    for j in range(8):
+        lanes = slice(256 * j, 256 * (j + 1))
+        partial[0, :, lanes] = (mixed[:, lanes] + mix_part(3, lanes)).astype(bf16)
 
     piece = [pl.ds(64 * at, 64) for at in range(4)]
     first_rows = [links.arrival(), links.arrival()]
-    for at in range(2):
-
-        @pl.loop(0, 4)
+    for at in range(4):
+
+        @pl.loop(0, 2)
         def _(step):
-            for start in (64 * at, 64 * at + 128):
+            for start in (32 * at, 32 * at + 128):
                 lines = pl.ds(pl.multiple_of(start + 16 * step, 16), 16)
                 mid = (
                     middle[lines, :].astype(f32) + rms_norm(partial[0, lines, :], gains[0])
@@ -463,8 +475,9 @@
                 middle[lines, :] = mid
                 rows[x, lines, :] = rms_norm(mid, gains[1]).astype(bf16)
 
-        for target, lines in ((x_up, piece[at]), (x_down, piece[2 + at])):
-            links.send(first_rows[at], rows.at[x, lines], rows.at[x, lines], **{X: target})
+        for target, start in ((x_up, 32 * at), (x_down, 32 * at + 128)):
+            lines = pl.ds(start, 32)
+            links.send(first_rows[at // 2], rows.at[x, lines], rows.at[x, lines], **{X: target})
     for gather in narrow:
         gather.line()
     for gather in (*wide, *narrow):
@@ -486,9 +499,9 @@
     for gather in wide:
         gather.arrive()
 
-    def gate_up(owner, slot):
+    def gate_up(owner, slot, tiles=range(11)):
         block = rows[owner]
-        for j in range(11):
+        for j in tiles:
             lanes = slice(128 * j, 128 * (j + 1))
             weights = jnp.concatenate(
                 [
@@ -513,9 +526,10 @@
             partial[to, lines, lanes] = part.astype(bf16)
 
     far.wait(rows.at[x_far])
-    gate_up(x_far, 2)
+    gate_up(x_far, 2, range(6))
     for gather in narrow:
         gather.end_line()
+    gate_up(x_far, 2, range(6, 11))
     for gather in narrow:
         gather.arrive()
     down(2, 1)
@@ -541,13 +555,15 @@
         links.send(last[at], partial.at[3, piece[2 + at]], final.at[1, piece[2 + at]], **{X: x_down})
     down(2, 0)
     last[2].wait(final.at[0])
-    for at in range(2):
-        last[at].wait(final.at[0, top])
+
+    @pl.loop(0, 2)
+    def _(at):
+        Arrival(links, last[0].at + at).wait(final.at[0, top])
 
         @pl.loop(0, 4)
         def _(step):
-            for start in (64 * at, 64 * at + 128):
-                lines = pl.ds(pl.multiple_of(start + 16 * step, 16), 16)
+            for start in (0, 128):
+                lines = pl.ds(pl.multiple_of(start + 64 * at + 16 * step, 16), 16)
                 branch = (
                     partial[0, lines, :].astype(f32)
                     + final[0, lines, :].astype(f32)
@@ -599,6 +615,7 @@
             pltpu.VMEM((4, 256, 256), bf16),
             pltpu.VMEM((128, 256), bf16),
             pltpu.VMEM((4, 256, 2048), bf16),
+            pltpu.VMEM((256, 2048), f32),
             pltpu.VMEM((256, 2048), bf16),
             pltpu.VMEM((2, 1024), f32),
             pltpu.VMEM((3, 1, 2048), f32),

time: 107 us -> 106 us (level); the launches traced: 106 us -> 106 us
  no operation moved by 1% of the time
where the time goes in v5:
time: 106 us
  Pallas kernels  105 us (99%)
    pallas_call x1, Pallas kernels, per_device(): pl.pallas_call(layer_kernel, out_shape=jax.ShapeDtypeStruct((256, 2048),...  105 us

profile of v5, /device:TPU:1, one launch (start us, length us, event | category | flops | bytes accessed | tf_op | source)
XLA Modules:
  0.0 106.2 jit_solution(13557762888526155673)
XLA Ops:
  0.0 105.3 %layer.1 = bf16[256,2048]{1,0:T(8,128)(2,1)S(1)} custom-call(bf16[1024,256]{1,0:T(8,128)(2,1)} %queries.1, bf16[1024,256]{1,0:T(8,128)(2,1)} %keys.1, bf16[1024,256]{1,0:T(8,128)(2,1)} %values.1, bf16[1024,256]{1,0:T(8,128)(2,1)} %gates.1, f32[2,1024]{1,0:T(2,128)} %bitcast.6, f32[2,128]{1,0:T(2,128)} %norm_gain.1, bf16[256,2048]{1,0:T(8,128)(2,1)} %out_weight.1, ...), custom_call_target="tpu_custom_call" | custom-call | tf_op jit(solution)/shard_map/layer/pallas_call | solution.py:588
  105.3 1.0 copy.16

commit v6 on v5

--- a/solution.py
+++ b/solution.py
@@ -13,7 +13,7 @@
 
 EPSILON = 1e-06
 MESH_ID = pl.DeviceIdType.MESH
-SENDS, ARRIVALS = 40, 48
+SENDS, ARRIVALS = 32, 50
 Z, Y, C, X = SP_TP
 
 
@@ -58,7 +58,7 @@
     def finish(self):
         for copy in self.copies[-SENDS:]:
             copy.wait_send()
-        assert self.arrivals <= ARRIVALS
+        assert self.arrivals == ARRIVALS, self.arrivals
 
 
 class PlaneGather:
@@ -434,12 +434,12 @@
         gather.pass_on()
     for gather in (wide[1], wide[0]):
         gather.line()
-    to_pass.wait(passing)
-    links.send(far_came, passing, regrouped.at[3, bottom], **{X: x_down})
     shared, shared_far = links.arrival(), links.arrival()
     weight_rest.wait(out_all.at[pl.ds(1, 2), pl.ds(0, 96)])
     near_half, far_half = out_all.at[pl.ds(1, 2), half_rows], out_all.at[3, half_rows]
     links.send(shared, near_half, near_half, **{C: other})
+    to_pass.wait(passing)
+    links.send(far_came, passing, regrouped.at[3, bottom], **{X: x_down})
     weight_far.finish()
     links.send(shared_far, far_half, far_half, **{C: other})
     for name in ("resid", "mix", "in", "out"):
@@ -513,9 +513,9 @@
             both = jnp.dot(block, weights, preferred_element_type=f32)
             hidden[slot, :, lanes] = (jax.nn.silu(both[:, :128]) * both[:, 128:]).astype(bf16)
 
-    def down(slot, to, lines=pl.ds(0, 256), extra=None):
+    def down(slot, to, lines=pl.ds(0, 256), extra=None, tiles=range(8)):
         block = hidden[slot, lines, :]
-        for j in range(8):
+        for j in tiles:
             weights = jnp.concatenate(
                 [down_all[j // 2, 2 * j % 4], down_all[j // 2, 2 * j % 4 + 1]], axis=1
             )
@@ -532,38 +532,42 @@
     gate_up(x_far, 2, range(6, 11))
     for gather in narrow:
         gather.arrive()
-    down(2, 1)
     relay_up, relay_down = links.arrival(), links.arrival()
-    links.send(relay_up, partial.at[1, top], relay.at[0], **{X: x_up})
-    links.send(relay_down, partial.at[1, bottom], relay.at[1], **{X: x_down})
+    for at in range(2):
+        down(2, 1, tiles=range(4 * at, 4 * at + 4))
+        lanes = pl.ds(1024 * at, 1024)
+        links.send(relay_up, partial.at[1, top, lanes], relay.at[0, :, lanes], **{X: x_up})
+        links.send(relay_down, partial.at[1, bottom, lanes], relay.at[1, :, lanes], **{X: x_down})
     nearby.wait(rows.at[x_up])
     gate_up(x_up, 0)
     down(0, 2, bottom)
-    last = [links.arrival() for _ in range(3)]
-    links.send(last[2], partial.at[2, bottom], final.at[0, bottom], **{X: x_up})
+    last = [links.arrival() for _ in range(5)]
+    links.send(last[4], partial.at[2, bottom], final.at[0, bottom], **{X: x_up})
     gate_up(x_down, 1)
     down(1, 3, top)
-    links.send(last[2], partial.at[3, top], final.at[1, top], **{X: x_down})
+    links.send(last[4], partial.at[3, top], final.at[1, top], **{X: x_down})
     gate_up(x, 2)
     relay_up.wait(relay.at[0])
     down(0, 2, top, 0)
-    for at in range(2):
-        links.send(last[at], partial.at[2, piece[at]], final.at[0, piece[at]], **{X: x_up})
+    for at in range(4):
+        lines = pl.ds(32 * at, 32)
+        links.send(last[at], partial.at[2, lines], final.at[0, lines], **{X: x_up})
     relay_down.wait(relay.at[1])
     down(1, 3, bottom, 1)
-    for at in range(2):
-        links.send(last[at], partial.at[3, piece[2 + at]], final.at[1, piece[2 + at]], **{X: x_down})
+    for at in range(4):
+        lines = pl.ds(128 + 32 * at, 32)
+        links.send(last[at], partial.at[3, lines], final.at[1, lines], **{X: x_down})
     down(2, 0)
-    last[2].wait(final.at[0])
-
-    @pl.loop(0, 2)
+    last[4].wait(final.at[0])
+
+    @pl.loop(0, 4)
     def _(at):
-        Arrival(links, last[0].at + at).wait(final.at[0, top])
-
-        @pl.loop(0, 4)
+        Arrival(links, last[0].at + at).wait(final.at[0, pl.ds(0, 64)])
+
+        @pl.loop(0, 2)
         def _(step):
             for start in (0, 128):
-                lines = pl.ds(pl.multiple_of(start + 64 * at + 16 * step, 16), 16)
+                lines = pl.ds(pl.multiple_of(start + 32 * at + 16 * step, 16), 16)
                 branch = (
                     partial[0, lines, :].astype(f32)
                     + final[0, lines, :].astype(f32)

time: 106 us -> 105 us (level)
    pallas_call x1, Pallas kernels: 105 us -> 104 us  [per_device(): pl.pallas_call(layer_kernel, out_shape=jax.ShapeDtypeStruct((256, 2048),...]
where the time goes in v6:
time: 105 us
  Pallas kernels  104 us (99%)
    pallas_call x1, Pallas kernels, per_device(): pl.pallas_call(layer_kernel, out_shape=jax.ShapeDtypeStruct((256, 2048),...  104 us

profile of v6, /device:TPU:1, one launch (start us, length us, event | category | flops | bytes accessed | tf_op | source)
XLA Modules:
  0.0 105.0 jit_solution(4785265314388732450)
XLA Ops:
  0.0 104.0 %layer.1 = bf16[256,2048]{1,0:T(8,128)(2,1)S(1)} custom-call(bf16[1024,256]{1,0:T(8,128)(2,1)} %queries.1, bf16[1024,256]{1,0:T(8,128)(2,1)} %keys.1, bf16[1024,256]{1,0:T(8,128)(2,1)} %values.1, bf16[1024,256]{1,0:T(8,128)(2,1)} %gates.1, f32[2,1024]{1,0:T(2,128)} %bitcast.6, f32[2,128]{1,0:T(2,128)} %norm_gain.1, bf16[256,2048]{1,0:T(8,128)(2,1)} %out_weight.1, ...), custom_call_target="tpu_custom_call" | custom-call | tf_op jit(solution)/shard_map/layer/pallas_call | solution.py:592
  104.0 1.0 copy.16

commit v7 on v6

--- a/solution.py
+++ b/solution.py
@@ -113,12 +113,11 @@
         self.give(self.j_down)
         self.give(self.j_up)
 
-    def end_line(self):
+    def end_line(self, at):
         far = lax.rem(self.j + 2, 4)
-        for at, arrival in enumerate(self.passed):
-            arrival.wait(self.at(pl.ds(0, 2), far))
-            for start in (0, 2):
-                self.give(far, pl.ds(start + at, 1))
+        self.passed[at].wait(self.at(pl.ds(0, 2), far))
+        for start in (0, 2):
+            self.give(far, pl.ds(start + at, 1))
 
     def arrive(self):
         self.across.wait(self.at(pl.ds(0, 4), pl.ds(0, 4)))
@@ -494,8 +493,9 @@
         links.send(nearby, rows.at[x, lines], rows.at[x, lines], **{X: target})
     for gather in narrow:
         gather.pass_line()
-    for gather in wide:
-        gather.end_line()
+    for at in range(2):
+        for gather in wide:
+            gather.end_line(at)
     for gather in wide:
         gather.arrive()
 
@@ -526,10 +526,11 @@
             partial[to, lines, lanes] = part.astype(bf16)
 
     far.wait(rows.at[x_far])
-    gate_up(x_far, 2, range(6))
-    for gather in narrow:
-        gather.end_line()
-    gate_up(x_far, 2, range(6, 11))
+    gate_up(x_far, 2, range(3))
+    for at in range(2):
+        for gather in narrow:
+            gather.end_line(at)
+    gate_up(x_far, 2, range(3, 11))
     for gather in narrow:
         gather.arrive()
     relay_up, relay_down = links.arrival(), links.arrival()

time: 105 us -> 105 us (level)
  no operation moved by 1% of the time
where the time goes in v7:
time: 105 us
  Pallas kernels  104 us (99%)
    pallas_call x1, Pallas kernels, per_device(): pl.pallas_call(layer_kernel, out_shape=jax.ShapeDtypeStruct((256, 2048),...  104 us

profile of v7, /device:TPU:1, one launch (start us, length us, event | category | flops | bytes accessed | tf_op | source)
XLA Modules:
  0.0 104.9 jit_solution(2836033951306987277)
XLA Ops:
  0.0 104.0 %layer.1 = bf16[256,2048]{1,0:T(8,128)(2,1)S(1)} custom-call(bf16[1024,256]{1,0:T(8,128)(2,1)} %queries.1, bf16[1024,256]{1,0:T(8,128)(2,1)} %keys.1, bf16[1024,256]{1,0:T(8,128)(2,1)} %values.1, bf16[1024,256]{1,0:T(8,128)(2,1)} %gates.1, f32[2,1024]{1,0:T(2,128)} %bitcast.6, f32[2,128]{1,0:T(2,128)} %norm_gain.1, bf16[256,2048]{1,0:T(8,128)(2,1)} %out_weight.1, ...), custom_call_target="tpu_custom_call" | custom-call | tf_op jit(solution)/shard_map/layer/pallas_call | solution.py:593
  104.0 1.0 copy.16

commit v8 on v7

--- a/solution.py
+++ b/solution.py
@@ -534,9 +534,9 @@
     for gather in narrow:
         gather.arrive()
     relay_up, relay_down = links.arrival(), links.arrival()
-    for at in range(2):
-        down(2, 1, tiles=range(4 * at, 4 * at + 4))
-        lanes = pl.ds(1024 * at, 1024)
+    for at in range(4):
+        down(2, 1, tiles=range(2 * at, 2 * at + 2))
+        lanes = pl.ds(512 * at, 512)
         links.send(relay_up, partial.at[1, top, lanes], relay.at[0, :, lanes], **{X: x_up})
         links.send(relay_down, partial.at[1, bottom, lanes], relay.at[1, :, lanes], **{X: x_down})
     nearby.wait(rows.at[x_up])

time: 105 us -> 105 us (level)
  no operation moved by 1% of the time
where the time goes in v8:
time: 105 us
  Pallas kernels  104 us (99%)
    pallas_call x1, Pallas kernels, per_device(): pl.pallas_call(layer_kernel, out_shape=jax.ShapeDtypeStruct((256, 2048),...  104 us

profile of v8, /device:TPU:1, one launch (start us, length us, event | category | flops | bytes accessed | tf_op | source)
XLA Modules:
  0.0 104.5 jit_solution(17484573094707018078)
XLA Ops:
  0.0 103.6 %layer.1 = bf16[256,2048]{1,0:T(8,128)(2,1)S(1)} custom-call(bf16[1024,256]{1,0:T(8,128)(2,1)} %queries.1, bf16[1024,256]{1,0:T(8,128)(2,1)} %keys.1, bf16[1024,256]{1,0:T(8,128)(2,1)} %values.1, bf16[1024,256]{1,0:T(8,128)(2,1)} %gates.1, f32[2,1024]{1,0:T(2,128)} %bitcast.6, f32[2,128]{1,0:T(2,128)} %norm_gain.1, bf16[256,2048]{1,0:T(8,128)(2,1)} %out_weight.1, ...), custom_call_target="tpu_custom_call" | custom-call | tf_op jit(solution)/shard_map/layer/pallas_call | solution.py:593
  103.6 1.0 copy.16
